TPU v7x, 32 devices: a whole 2x2x4 slice. The times are simulated.
32 devices in a mesh: sp: 8 (over z, x), tp: 4 (over y, core).
Axes of the slice: x: 2, y: 2, z: 4, core: 2. Of those that a mesh axis runs over, the one named last changes fastest.
Arguments:
- query_maps: bfloat16 [1536, 1024], P('sp', 'tp'), may hold values from -6 to 6
- key_maps: bfloat16 [1536, 512], P('sp', 'tp'), may hold values from -6 to 6
- value_rows: bfloat16 [1536, 512], P('sp', 'tp'), may hold values from -6 to 6
- mix_lambda: float32 [8], P('tp'), may hold values from 0.3 to 0.8
- head_gain: float32 [128], replicated, may hold values from 0.1 to 1.9
- out_weight: bfloat16 [1024, 2048], replicated, may hold values from -0.1875 to 0.1875
- residual: bfloat16 [1536, 2048], P(('sp', 'tp')), may hold values from -6 to 6
- norm_gain: float32 [2048], replicated, may hold values from 0.1 to 1.9
- routes: int32 [1536, 4], P('sp'), may hold values from 0 to 7, all different within a row; in each aligned block of 48 rows (0 to 47, 48 to 95, ...) at most 48 rows name the same one
- route_weight: float32 [1536, 4], P(('sp', 'tp')), may hold values from 0.3 to 1.5
- expert_gate: bfloat16 [8, 2048, 1024], P('sp', None, 'tp'), may hold values from -0.125 to 0.125
- expert_up: bfloat16 [8, 2048, 1024], P('sp', None, 'tp'), may hold values from -0.125 to 0.125
- expert_down: bfloat16 [8, 1024, 2048], P('sp', 'tp'), may hold values from -0.1875 to 0.1875
- shared_gate: bfloat16 [2048, 1024], P(None, 'tp'), may hold values from -0.125 to 0.125
- shared_up: bfloat16 [2048, 1024], P(None, 'tp'), may hold values from -0.125 to 0.125
- shared_down: bfloat16 [1024, 2048], P('tp'), may hold values from -0.1875 to 0.1875
Outputs:
- mixed: bfloat16 [1536, 2048], P(('sp', 'tp'))
Inputs may be any that keep to these rules, and one draw needn't show every extreme that they name: `routes`: the 4 experts of a token are different. In each aligned block of 48 tokens (the tokens of one device after the attention) no expert is named more than 48 times, a bound that some expert reaches in some blocks.
All inputs are finite; a program needn't handle non-finite values.
Results may differ from a plain program's by a relative error of at most 0.018.
Values may be sent and summed in bfloat16 or wider, within the bound.
A program may use at most 128 MiB of HBM per device.

v0:
```python
from functools import partial

import jax
import jax.numpy as jnp
from jax import lax
from jax.experimental import pallas as pl
from jax.experimental.pallas import tpu as pltpu
from jax.sharding import PartitionSpec as P


norm_eps = 1e-06
lowest_score = -1e30


def slot_targets(block_routes, experts, capacity):
    flat_routes = block_routes.reshape(-1)
    onehot = (flat_routes[:, None] == jnp.arange(experts, dtype=jnp.int32)[None, :]).astype(
        jnp.int32
    )
    earlier = jnp.cumsum(onehot, axis=0) - onehot
    return flat_routes * capacity + jnp.sum(earlier * onehot, axis=1)


def build_buffer(token_rows, block_routes, experts, capacity):
    targets = slot_targets(block_routes, experts, capacity)
    row_total = block_routes.shape[0]
    route_count = block_routes.shape[1]
    source_row = jnp.arange(row_total * route_count, dtype=jnp.int32) // route_count
    holder = jnp.full((experts * capacity,), row_total, jnp.int32).at[targets].set(source_row)
    padded = jnp.concatenate(
        [token_rows, jnp.zeros((1, token_rows.shape[1]), token_rows.dtype)], axis=0
    )
    return (padded[holder], targets)


def attention_block(carried, queries, key_block, value_block, score_scale):
    run_max, run_sum, accumulated = carried
    kv_local = run_max.shape[0]
    key_heads = key_block.reshape(key_block.shape[0], kv_local, 2, -1)
    value_heads = value_block.reshape(value_block.shape[0], kv_local, -1)
    scores = (
        jnp.einsum("qagcd,racd->agcqr", queries, key_heads, preferred_element_type=jnp.float32)
        * score_scale
    )
    new_max = jnp.maximum(run_max, jnp.max(scores, axis=-1))
    rescale = jnp.exp(run_max - new_max)
    weights = jnp.exp(scores - new_max[..., None])
    run_sum = run_sum * rescale + jnp.sum(weights, axis=-1)
    update = jnp.einsum(
        "agcqr,rae->agcqe",
        weights.astype(jnp.bfloat16),
        value_heads,
        preferred_element_type=jnp.float32,
    )
    return (new_max, run_sum, accumulated * rescale[..., None] + update)


def fold_keys(carried, pieces, first_row, queries, score_scale):
    key_piece, value_piece = pieces
    total_rows = key_piece.shape[0]
    block_rows = total_rows
    for candidate in (2048, 1024, 512):
        if total_rows % candidate == 0:
            block_rows = candidate
            break
    block_count = total_rows // block_rows

    def block_step(block_index, running):
        start_row = block_index * block_rows
        return attention_block(
            running,
            queries,
            lax.dynamic_slice_in_dim(key_piece, start_row, block_rows, 0),
            lax.dynamic_slice_in_dim(value_piece, start_row, block_rows, 0),
            score_scale,
        )

    return lax.fori_loop(0, block_count, block_step, carried)


def whole_experts(arrived, whole_gate, whole_up, whole_down, senders, capacity, groups):
    local_experts = whole_gate.shape[0]
    width = arrived.shape[-1]
    rows_in = arrived.reshape(senders, local_experts, capacity, width)
    gate_value = jnp.einsum(
        "sjtd,jdf->sjtf", rows_in, whole_gate, preferred_element_type=jnp.float32
    )
    up_value = jnp.einsum("sjtd,jdf->sjtf", rows_in, whole_up, preferred_element_type=jnp.float32)
    hidden = (jax.nn.silu(gate_value) * up_value).astype(jnp.bfloat16)
    hidden_units = hidden.shape[-1]
    hidden = hidden.reshape(senders, local_experts, capacity, groups, hidden_units // groups)
    down_groups = whole_down.reshape(local_experts, groups, hidden_units // groups, width)
    group_sums = jnp.einsum(
        "sjtgf,jgfd->sjtgd", hidden, down_groups, preferred_element_type=jnp.float32
    )
    group_sums = lax.optimization_barrier(group_sums.astype(jnp.bfloat16)).astype(jnp.float32)
    return (
        jnp.sum(group_sums, axis=3)
        .astype(jnp.bfloat16)
        .reshape(senders * local_experts * capacity, width)
    )


def body(
    query_maps,
    key_maps,
    value_rows,
    mix_lambda,
    head_gain,
    out_weight,
    residual,
    norm_gain,
    routes,
    route_weight,
    expert_gate,
    expert_up,
    expert_down,
    shared_gate,
    shared_up,
    shared_down,
):
    local_heads = mix_lambda.shape[0]
    head_width = head_gain.shape[0]
    kv_local = value_rows.shape[1] // head_width
    head_group = local_heads // kv_local
    head_dim = key_maps.shape[1] // (2 * kv_local)
    token_count = query_maps.shape[0]
    queries = query_maps.reshape(token_count, kv_local, head_group, 2, head_dim)
    start_max = jnp.full((kv_local, head_group, 2, token_count), lowest_score, jnp.float32)
    start_sum = jnp.zeros((kv_local, head_group, 2, token_count), jnp.float32)
    start_values = jnp.zeros((kv_local, head_group, 2, token_count, head_width), jnp.float32)
    folder = partial(fold_keys, queries=queries, score_scale=head_dim ** (-0.5))
    _, run_sum, accumulated = folder(
        (start_max, start_sum, start_values),
        (
            lax.all_gather(key_maps, "sp", axis=0, tiled=True),
            lax.all_gather(value_rows, "sp", axis=0, tiled=True),
        ),
        jnp.int32(0),
    )
    normalized = accumulated / run_sum[..., None]
    lambdas = mix_lambda.reshape(kv_local, head_group, 1, 1)
    difference = normalized[:, :, 0] - lambdas * normalized[:, :, 1]
    inverse_rms = lax.rsqrt(jnp.mean(difference * difference, axis=-1, keepdims=True) + norm_eps)
    head_scaled = (difference * inverse_rms * head_gain).astype(jnp.bfloat16)
    attended = jnp.transpose(head_scaled, (2, 0, 1, 3)).reshape(
        token_count, local_heads * head_width
    )
    columns = lax.axis_size("tp")
    column = lax.axis_index("tp")
    rows_dev = token_count // columns
    own_rows = lax.dynamic_slice_in_dim(
        out_weight, column * attended.shape[1], attended.shape[1], 0
    )
    projected = lax.psum_scatter(
        jnp.dot(attended, own_rows, preferred_element_type=jnp.float32).astype(jnp.bfloat16),
        "tp",
        scatter_dimension=0,
        tiled=True,
    ).astype(jnp.float32)
    stream = (residual.astype(jnp.float32) + projected).astype(jnp.bfloat16)
    stream_wide = stream.astype(jnp.float32)
    stream_rms = lax.rsqrt(jnp.mean(stream_wide * stream_wide, axis=1, keepdims=True) + norm_eps)
    normed = (stream_wide * stream_rms * norm_gain).astype(jnp.bfloat16)
    senders = lax.axis_size("sp")
    local_experts = expert_gate.shape[0]
    experts = senders * local_experts
    route_count = routes.shape[1]
    capacity = max(2, 2 * rows_dev * route_count // experts)
    local_routed = None
    whole_gate, whole_up, whole_down = (
        lax.all_gather(expert_gate, "tp", axis=2, tiled=True),
        lax.all_gather(expert_up, "tp", axis=2, tiled=True),
        lax.all_gather(expert_down, "tp", axis=1, tiled=True),
    )
    own_routes = lax.dynamic_slice_in_dim(routes, column * rows_dev, rows_dev, 0)
    buffer, targets = build_buffer(normed, own_routes, experts, capacity)
    arrived = lax.all_to_all(buffer, "sp", split_axis=0, concat_axis=0, tiled=True)
    local_routed = whole_experts(
        arrived, whole_gate, whole_up, whole_down, senders, capacity, columns
    )
    shared_rows = lax.all_gather(normed[None], "tp", axis=0, tiled=True)
    shared_in = shared_rows
    shared_in = shared_in.reshape(1 * lax.axis_size("tp") * rows_dev, shared_in.shape[-1])
    shared_hidden = (
        jax.nn.silu(jnp.dot(shared_in, shared_gate, preferred_element_type=jnp.float32))
        * jnp.dot(shared_in, shared_up, preferred_element_type=jnp.float32)
    ).astype(jnp.bfloat16)
    shared_out = jnp.dot(shared_hidden, shared_down, preferred_element_type=jnp.float32)
    pieces = shared_out.reshape(1 * lax.axis_size("tp"), rows_dev, shared_out.shape[-1])
    terms_out = pieces.astype(jnp.bfloat16)
    summed = (
        lax.psum_scatter(
            lax.optimization_barrier(terms_out).astype(jnp.float32).astype(jnp.bfloat16),
            "tp",
            scatter_dimension=0,
            tiled=True,
        )
        .astype(jnp.float32)[0]
        .astype(jnp.bfloat16)
    )
    returned = lax.all_to_all(local_routed, "sp", split_axis=0, concat_axis=0, tiled=True)
    picked = (
        returned[targets].reshape(rows_dev, route_count, returned.shape[-1]).astype(jnp.float32)
    )
    routed_sum = jnp.sum(route_weight[:, :, None] * picked, axis=1)
    return (stream_wide + summed.astype(jnp.float32) + routed_sum).astype(jnp.bfloat16)


MESH = pl.DeviceIdType.MESH


def peer_barrier(peers):
    barrier = pltpu.get_barrier_semaphore()
    for peer in peers:
        pl.semaphore_signal(barrier, inc=1, device_id=peer, device_id_type=MESH)
    pl.semaphore_wait(barrier, len(peers))


def remote(src, dst, send_sem, recv_sem, peer):
    return pltpu.make_async_remote_copy(
        src_ref=src,
        dst_ref=dst,
        send_sem=send_sem,
        recv_sem=recv_sem,
        device_id=peer,
        device_id_type=MESH,
    )


def grid_place(sp):
    s = lax.axis_index("sp")
    t = lax.axis_index("tp")
    return s, t, s // 2, s % 2, sp // 2


def gather_kernel(sp, tp, count, with_tp, *refs):
    ins, refs = refs[:count], refs[count:]
    outs, refs = refs[:count], refs[count:]
    if with_tp:
        tp_out, refs = refs[0], refs[1:]
    send_sem, recv_sem, local_sem = refs[:3]
    s, t, z, x, depth = grid_place(sp)
    line = [(lax.rem(z + k, depth) * 2 + x, t) for k in range(1, depth)]
    across = (z * 2 + (1 - x), t)
    columns = [(s, lax.rem(t + k, tp)) for k in range(1, tp)] if with_tp else []
    peer_barrier(line + [across] + columns)
    copies = []
    arrivals = []
    for i in range(count):
        for k in (1, 3, 2) if depth == 4 else range(1, depth):
            copy = remote(
                ins[i], outs[i].at[s], send_sem.at[i, k], recv_sem.at[i, k], line[k - 1]
            )
            copy.start()
            copies.append(copy)
            arrivals.append((k, i, copy))
    for i in range(count):
        copy = remote(
            ins[i], outs[i].at[s], send_sem.at[i, depth], recv_sem.at[i, depth], across
        )
        copy.start()
        copies.append(copy)
    side = []
    if with_tp:
        for k in range(1, tp):
            copy = remote(
                ins[0],
                tp_out.at[t],
                send_sem.at[0, 2 * depth + k],
                recv_sem.at[0, 2 * depth + k],
                columns[k - 1],
            )
            copy.start()
            side.append(copy)
        own = pltpu.make_async_copy(ins[0], tp_out.at[t], local_sem.at[count])
        own.start()
    locals_ = []
    for i in range(count):
        copy = pltpu.make_async_copy(ins[i], outs[i].at[s], local_sem.at[i])
        copy.start()
        locals_.append(copy)
    order = {1: 0, 3: 1, 2: 2}
    arrivals.sort(key=lambda item: (order.get(item[0], item[0]), item[1]))
    for k, i, copy in arrivals:
        copy.wait_recv()
        origin = lax.rem(z + depth - k, depth) * 2 + x
        relay = remote(
            outs[i].at[origin],
            outs[i].at[origin],
            send_sem.at[i, depth + k],
            recv_sem.at[i, depth + k],
            across,
        )
        relay.start()
        side.append(relay)
    for _, _, copy in arrivals:
        copy.wait_send()
    for copy in copies:
        if not any(copy is entry[2] for entry in arrivals):
            copy.wait()
    for copy in side:
        copy.wait()
    for copy in locals_:
        copy.wait()
    if with_tp:
        own.wait()


def gather_sp(arrays, sp, tp, with_tp, collective_id):
    count = len(arrays)
    depth = sp // 2
    shapes = [jax.ShapeDtypeStruct((sp,) + a.shape, a.dtype) for a in arrays]
    if with_tp:
        shapes.append(jax.ShapeDtypeStruct((tp,) + arrays[0].shape, arrays[0].dtype))
    slots = 2 * depth + tp
    return pl.pallas_call(
        partial(gather_kernel, sp, tp, count, with_tp),
        out_shape=tuple(shapes),
        in_specs=[pl.BlockSpec(memory_space=pltpu.VMEM)] * count,
        out_specs=tuple([pl.BlockSpec(memory_space=pltpu.VMEM)] * len(shapes)),
        scratch_shapes=[
            pltpu.SemaphoreType.DMA((count, slots)),
            pltpu.SemaphoreType.DMA((count, slots)),
            pltpu.SemaphoreType.DMA((count + 1,)),
        ],
        compiler_params=pltpu.CompilerParams(
            collective_id=collective_id,
            has_side_effects=True,
            vmem_limit_bytes=16 * 1024 * 1024,
        ),
        cost_estimate=pl.CostEstimate(flops=0, bytes_accessed=40_000_000, transcendentals=0),
    )(*arrays)


def heads_kernel(tp, x_ref, out_ref, send_sem, recv_sem, local_sem):
    s = lax.axis_index("sp")
    t = lax.axis_index("tp")
    width = x_ref.shape[1]
    rows = out_ref.shape[0]
    targets = [lax.rem(t + k, tp) for k in range(1, tp)]
    peer_barrier([(s, target) for target in targets])
    mine = pl.ds(pl.multiple_of(t * width, width), width)
    copies = []
    for k, target in zip(range(1, tp), targets):
        copy = remote(
            x_ref.at[pl.ds(pl.multiple_of(target * rows, rows), rows)],
            out_ref.at[:, mine],
            send_sem.at[k],
            recv_sem.at[k],
            (s, target),
        )
        copy.start()
        copies.append(copy)
    own = pltpu.make_async_copy(
        x_ref.at[pl.ds(pl.multiple_of(t * rows, rows), rows)], out_ref.at[:, mine], local_sem
    )
    own.start()
    for copy in copies:
        copy.wait()
    own.wait()


def exchange_heads(attended, tp, collective_id):
    tokens, width = attended.shape
    return pl.pallas_call(
        partial(heads_kernel, tp),
        out_shape=jax.ShapeDtypeStruct((tokens // tp, tp * width), attended.dtype),
        in_specs=[pl.BlockSpec(memory_space=pltpu.VMEM)],
        out_specs=pl.BlockSpec(memory_space=pltpu.VMEM),
        scratch_shapes=[
            pltpu.SemaphoreType.DMA((tp,)),
            pltpu.SemaphoreType.DMA((tp,)),
            pltpu.SemaphoreType.DMA,
        ],
        compiler_params=pltpu.CompilerParams(
            collective_id=collective_id,
            has_side_effects=True,
            vmem_limit_bytes=16 * 1024 * 1024,
        ),
        cost_estimate=pl.CostEstimate(flops=0, bytes_accessed=5_000_000, transcendentals=0),
    )(attended)


def moe_kernel(sp, *refs):
    normed_ref, stream_ref, weight_ref = refs[:3]
    sources = refs[3:17]
    out_ref = refs[17]
    gate, up, down, sgate, sup, sdown = refs[18:24]
    rows, hid_own, hid_out, hid_in, parts, xin, zout, zin, sout, sin = refs[24:34]
    zs, zr, xs, xr, ys, yr, hs, hr, os_, or_, rs, rr, ss, sr, wsem = refs[34:]
    s, t, z, x, depth = grid_place(sp)
    count, width = normed_ref.shape
    quarter = sources[0].shape[1]
    y, c = t // 2, t % 2
    across = (z * 2 + (1 - x), t)
    mirror = (s, (1 - y) * 2 + c)
    line = [(lax.rem(z + k, depth) * 2 + x, t) for k in range(1, depth)]
    first, second = pl.ds(0, quarter), pl.ds(quarter, quarter)
    places = (
        gate.at[:, first],
        gate.at[:, second],
        up.at[:, first],
        up.at[:, second],
        sgate.at[:, first],
        sgate.at[:, second],
        sup.at[:, first],
        sup.at[:, second],
        sdown.at[first],
        sdown.at[second],
    ) + tuple(down.at[pl.ds(q * quarter, quarter)] for q in range(4))
    loads = [
        pltpu.make_async_copy(source, place, wsem.at[n])
        for n, (source, place) in enumerate(zip(sources, places))
    ]
    for load in loads:
        load.start()
    peer_barrier(line + [across, mirror])

    z_rows, x_rows, y_rows, hids, x_outs, z_outs = {}, {}, {}, {}, {}, {}

    def send_y(j, xx, source):
        y_rows[j, xx] = remote(
            source, rows.at[1, j, xx], ys.at[2 * j + xx], yr.at[2 * j + xx], mirror
        )
        y_rows[j, xx].start()

    def send_x(j, source):
        x_rows[j] = remote(source, rows.at[0, j, 1], xs.at[j], xr.at[j], across)
        x_rows[j].start()

    order = [0, 1, 3, 2] if depth == 4 else list(range(depth))
    send_y(0, 0, normed_ref)
    send_x(0, normed_ref)
    for j in order[1:]:
        k = depth - j
        z_rows[j] = remote(
            normed_ref, rows.at[0, j, 0], zs.at[k - 1], zr.at[k - 1], line[k - 1]
        )
        z_rows[j].start()
    rows[0, 0, 0] = normed_ref[...]

    def hidden_of(block, gate_buf, up_buf):
        gate_value = jnp.dot(block, gate_buf[...], preferred_element_type=jnp.float32)
        up_value = jnp.dot(block, up_buf[...], preferred_element_type=jnp.float32)
        return (jax.nn.silu(gate_value) * up_value).astype(jnp.bfloat16)

    def relay(j):
        if j == 0:
            return
        z_rows[j].wait_recv()
        send_x(j, rows.at[0, j, 0])
        send_y(j, 0, rows.at[0, j, 0])

    def own_plane(j):
        x_rows[j].wait_recv()
        send_y(j, 1, rows.at[0, j, 1])
        if j == 0:
            for load in loads[:4]:
                load.wait()
        hid_own[j] = hidden_of(rows[0, j].reshape(2 * count, width), gate, up)

    def other_plane(j):
        if j != 0:
            y_rows[j, 0].wait_recv()
        y_rows[j, 1].wait_recv()
        hid_out[j] = hidden_of(rows[1, j].reshape(2 * count, width), gate, up)
        hids[j] = remote(hid_out.at[j], hid_in.at[j], hs.at[j], hr.at[j], mirror)
        hids[j].start()

    def finish_down(j):
        if j == 0:
            for load in loads[10:]:
                load.wait()
        hids[j].wait_recv()
        half = hid_own.shape[2]
        value = jnp.dot(
            hid_own[j], down[pl.ds(0, half)], preferred_element_type=jnp.float32
        ) + jnp.dot(hid_in[j], down[pl.ds(half, half)], preferred_element_type=jnp.float32)
        base = lax.rem(z + j, depth) * 2
        parts[j, 1] = (value[count:] * weight_ref[base + 1 - x]).astype(jnp.bfloat16)
        x_outs[j] = remote(parts.at[j, 1], xin.at[j], os_.at[j], or_.at[j], across)
        x_outs[j].start()
        parts[j, 0] = (value[:count] * weight_ref[base + x]).astype(jnp.bfloat16)

    def fold(j):
        x_outs[j].wait_recv()
        if j == 0:
            return
        zout[j - 1] = (parts[j, 0].astype(jnp.float32) + xin[j].astype(jnp.float32)).astype(
            jnp.bfloat16
        )
        z_outs[j] = remote(
            zout.at[j - 1], zin.at[j - 1], rs.at[j - 1], rr.at[j - 1], line[j - 1]
        )
        z_outs[j].start()

    relay(order[1])
    own_plane(order[0])
    y_rows[0, 0].wait_recv()
    for load in loads[4:10]:
        load.wait()
    pair = jnp.concatenate([normed_ref[...], rows[1, 0, 0]], axis=0)
    shared = jnp.dot(
        hidden_of(pair, sgate, sup), sdown[...], preferred_element_type=jnp.float32
    )
    sout[...] = shared[count:].astype(jnp.bfloat16)
    shared_copy = remote(sout, sin, ss, sr, mirror)
    shared_copy.start()
    total = stream_ref[...].astype(jnp.float32) + shared[:count]
    relay(order[2])
    own_plane(order[1])
    other_plane(order[0])
    relay(order[3])
    own_plane(order[2])
    other_plane(order[1])
    finish_down(order[0])
    own_plane(order[3])
    other_plane(order[2])
    finish_down(order[1])
    fold(order[0])
    other_plane(order[3])
    finish_down(order[2])
    fold(order[1])
    finish_down(order[3])
    fold(order[2])
    fold(order[3])
    shared_copy.wait_recv()
    total = total + sin[...].astype(jnp.float32)
    total = total + parts[0, 0].astype(jnp.float32) + xin[0].astype(jnp.float32)
    for j in order[1:]:
        z_outs[j].wait_recv()
        total = total + zin[j - 1].astype(jnp.float32)
    out_ref[...] = total.astype(out_ref.dtype)
    for group in (z_rows, x_rows, y_rows, hids, x_outs, z_outs):
        for copy in group.values():
            copy.wait_send()
    shared_copy.wait_send()


def run_moe(normed, stream, weights, sources, sp, collective_id):
    count, width = normed.shape
    depth = sp // 2
    quarter = sources[0].shape[1]
    half = 2 * quarter
    vmem = pl.BlockSpec(memory_space=pltpu.VMEM)

    def dma(n):
        return [pltpu.SemaphoreType.DMA((n,))] * 2

    bf16 = jnp.bfloat16
    return pl.pallas_call(
        partial(moe_kernel, sp),
        out_shape=jax.ShapeDtypeStruct((count, width), bf16),
        in_specs=[vmem] * 3 + [pl.BlockSpec(memory_space=pl.ANY)] * len(sources),
        out_specs=vmem,
        scratch_shapes=[
            pltpu.VMEM((width, half), bf16),
            pltpu.VMEM((width, half), bf16),
            pltpu.VMEM((2 * half, width), bf16),
            pltpu.VMEM((width, half), bf16),
            pltpu.VMEM((width, half), bf16),
            pltpu.VMEM((half, width), bf16),
            pltpu.VMEM((2, depth, 2, count, width), bf16),
            pltpu.VMEM((depth, 2 * count, half), bf16),
            pltpu.VMEM((depth, 2 * count, half), bf16),
            pltpu.VMEM((depth, 2 * count, half), bf16),
            pltpu.VMEM((depth, 2, count, width), bf16),
            pltpu.VMEM((depth, count, width), bf16),
            pltpu.VMEM((depth - 1, count, width), bf16),
            pltpu.VMEM((depth - 1, count, width), bf16),
            pltpu.VMEM((count, width), bf16),
            pltpu.VMEM((count, width), bf16),
        ]
        + dma(depth - 1)
        + dma(depth)
        + dma(2 * depth)
        + dma(depth)
        + dma(depth)
        + dma(depth - 1)
        + [pltpu.SemaphoreType.DMA] * 2
        + [pltpu.SemaphoreType.DMA((len(sources),))],
        compiler_params=pltpu.CompilerParams(
            collective_id=collective_id,
            has_side_effects=True,
            vmem_limit_bytes=44 * 1024 * 1024,
        ),
        cost_estimate=pl.CostEstimate(
            flops=12 * depth * count * width * half * 3,
            bytes_accessed=30_000_000,
            transcendentals=0,
        ),
    )(normed, stream, weights, *sources)


def dense_body(
    query_maps,
    key_maps,
    value_rows,
    mix_lambda,
    head_gain,
    out_weight,
    residual,
    norm_gain,
    routes,
    route_weight,
    expert_gate,
    expert_up,
    expert_down,
    shared_gate,
    shared_up,
    shared_down,
):
    sp = lax.axis_size("sp")
    tp = lax.axis_size("tp")
    s = lax.axis_index("sp")
    t = lax.axis_index("tp")

    def swapped(array, step):
        return lax.ppermute(array, "tp", [(i, i ^ step) for i in range(tp)])

    own_gate, own_up, own_down = expert_gate[0], expert_up[0], expert_down[0]
    far_down = swapped(own_down, 2)
    near_gate = swapped(own_gate, 1)
    near_up = swapped(own_up, 1)
    near_sgate = swapped(shared_gate, 1)
    near_sup = swapped(shared_up, 1)
    near_sdown = swapped(shared_down, 1)
    near_down = swapped(own_down, 1)

    local_heads = mix_lambda.shape[0]
    head_width = head_gain.shape[0]
    kv_local = value_rows.shape[1] // head_width
    head_group = local_heads // kv_local
    head_dim = key_maps.shape[1] // (2 * kv_local)
    token_count = query_maps.shape[0]
    rows_dev = token_count // tp
    experts = sp

    own_routes = lax.dynamic_slice_in_dim(routes, t * rows_dev, rows_dev, 0)
    named = own_routes[None, :, :] == jnp.arange(experts, dtype=jnp.int32)[:, None, None]
    table = jnp.sum(jnp.where(named, route_weight[None], 0.0), axis=2)
    lanes = -(-rows_dev // 128) * 128
    table = jnp.pad(table, ((0, 0), (0, lanes - rows_dev)))

    key_all, value_all, tables = gather_sp([key_maps, value_rows, table], sp, tp, False, 1)
    key_all = key_all.reshape(sp * token_count, -1)
    value_all = value_all.reshape(sp * token_count, -1)
    weights = lax.dynamic_index_in_dim(tables, s, 1, False)[:, :rows_dev, None]

    queries = query_maps.reshape(token_count, kv_local, head_group, 2, head_dim)
    start_max = jnp.full((kv_local, head_group, 2, token_count), lowest_score, jnp.float32)
    start_sum = jnp.zeros((kv_local, head_group, 2, token_count), jnp.float32)
    start_values = jnp.zeros((kv_local, head_group, 2, token_count, head_width), jnp.float32)
    _, run_sum, accumulated = fold_keys(
        (start_max, start_sum, start_values),
        (key_all, value_all),
        jnp.int32(0),
        queries,
        head_dim ** (-0.5),
    )
    normalized = accumulated / run_sum[..., None]
    lambdas = mix_lambda.reshape(kv_local, head_group, 1, 1)
    difference = normalized[:, :, 0] - lambdas * normalized[:, :, 1]
    inverse_rms = lax.rsqrt(jnp.mean(difference * difference, axis=-1, keepdims=True) + norm_eps)
    head_scaled = (difference * inverse_rms * head_gain).astype(jnp.bfloat16)
    attended = jnp.transpose(head_scaled, (2, 0, 1, 3)).reshape(
        token_count, local_heads * head_width
    )
    attended = exchange_heads(attended, tp, 2)
    projected = jnp.dot(attended, out_weight, preferred_element_type=jnp.float32)
    stream = (residual.astype(jnp.float32) + projected).astype(jnp.bfloat16)
    stream_wide = stream.astype(jnp.float32)
    stream_rms = lax.rsqrt(jnp.mean(stream_wide * stream_wide, axis=1, keepdims=True) + norm_eps)
    normed = (stream_wide * stream_rms * norm_gain).astype(jnp.bfloat16)
    far_near_down = swapped(far_down, 1)
    return run_moe(
        normed,
        stream,
        weights,
        (
            own_gate,
            near_gate,
            own_up,
            near_up,
            shared_gate,
            near_sgate,
            shared_up,
            near_sup,
            shared_down,
            near_sdown,
            own_down,
            near_down,
            far_down,
            far_near_down,
        ),
        sp,
        4,
    )


def solution(mesh):
    in_specs = (
        P("sp", "tp"),
        P("sp", "tp"),
        P("sp", "tp"),
        P("tp"),
        P(),
        P(),
        P(("sp", "tp"), None),
        P(),
        P("sp", None),
        P(("sp", "tp"), None),
        P("sp", None, "tp"),
        P("sp", None, "tp"),
        P("sp", "tp", None),
        P(None, "tp"),
        P(None, "tp"),
        P("tp", None),
    )
    out_specs = P(("sp", "tp"), None)
    sp, tp = mesh.shape["sp"], mesh.shape["tp"]

    def chosen(*args):
        route_count = args[8].shape[1]
        experts = sp * args[10].shape[0]
        rows_dev = args[6].shape[0]
        whole_blocks = 2 * rows_dev * route_count >= experts * rows_dev
        dense = whole_blocks and args[10].shape[0] == 1 and sp == 8 and tp == 4
        if not dense:
            return body(*args)
        return dense_body(*args)

    return jax.shard_map(
        chosen, mesh=mesh, in_specs=in_specs, out_specs=out_specs, check_vma=False
    )
```

profile of v0, /device:TPU:0, one launch (start us, length us, event | category | flops | bytes accessed | tf_op | source)
XLA Modules:
  0.0 118.7 jit_solution(4812151195392261158)
XLA Ops:
  0.0 3.0 %collective-permute-start.6 = (bf16[256,2048]{1,0:T(8,128)(2,1)}, bf16[256,2048]{1,0:T(8,128)(2,1)}, u32[]{:S(2)}, u32[]{:S(2)}) collective-permute-start(bf16[256,2048]{1,0:T(8,128)(2,1)} %bitcast.118), channel_id=1, source_target_pairs={{0,2},{1,3},{2,0},{3,1},{4,6},{5,7},{6,4},{7,5},{8,10},{9,11},{10,... | collective-permute-start | bytes 3145736 | tf_op jit(solution)/shard_map/ppermute | solution.py:620
  3.0 0.5 collective-permute-start
  3.5 0.5 collective-permute-start.2
  4.0 1.0 copy.38
  5.1 0.7 select_reduce_fusion
  5.8 0.8 copy-done.1
  6.6 0.8 copy-done.2
  7.4 18.0 %shard_map.154 = (bf16[8,192,128]{2,1,0:T(8,128)(2,1)S(1)}, bf16[8,192,128]{2,1,0:T(8,128)(2,1)S(1)}, f32[8,8,128]{2,1,0:T(8,128)S(1)}) custom-call(bf16[192,128]{1,0:T(8,128)(2,1)S(1)} %copy-done.1, bf16[192,128]{1,0:T(8,128)(2,1)S(1)} %copy-done.2, f32[8,128]{1,0:T(8,128)S(1)} %pad.4.refs_2_), custom_call_target="tpu_custom_call" | custom-call | bytes 40000000 | tf_op jit(solution)/shard_map/pallas_call | solution.py:317
  25.5 9.0 %while.18 = (s32[]{:T(128)}, f32[1,2,2,192]{3,1,2,0:T(2,128)S(1)}, f32[1,2,2,192]{3,1,2,0:T(2,128)S(1)}, f32[1,2,2,192,128]{4,3,2,1,0:T(8,128)}, bf16[1536,128]{...) while((s32[]{:T(128)}, f32[1,2,2,192]{3,1,2,0:T(2,128)S(1)}, ...), condition=%wide.region_4.5_spmd.clone, body=%wide.region_1.4_spmd.clone.sunk | while | flops 153260544 | bytes 6443191 | solution.py:78
  25.7 0.5 bitcast_reduce_fusion.2
  26.2 0.4 fusion.31
  26.7 1.1 fusion.32
  28.0 0.5 bitcast_reduce_fusion.2
  28.5 0.4 fusion.31
  29.0 2.1 %fusion.32 = f32[1,2,2,192,128]{4,3,2,1,0:T(8,128)} fusion(bf16[2,2,192,512]{3,2,0,1:T(8,128)(2,1)S(1)} %get-tuple-element.258, f32[1,2,2,192,128]{4,3,2,1,0:T(8,128)} %get-tuple-element.274, f32[2,2,192]{2,1,0:T(2,128)S(1)} %copy.59, pred[]{:T(512)S(6)} %compare.4, bf16[1536,128]{1,0:T(8,128)(2,1)S(1)} %get-tuple-element.288, s32[]{:T(128)S(6)} %select_n.25), kind=kOutput, calls=%fused_computation.7.clone.1 | convolution fusion | flops 100958208 | bytes 1708037 | tf_op jit(solution)/shard_map/while/body/eval_jaxpr/agcqr,rae->agcqe/dot_general | solution.py:49
  31.3 0.5 bitcast_reduce_fusion.2
  31.8 0.4 fusion.31
  32.3 2.1 %fusion.32 = f32[1,2,2,192,128]{4,3,2,1,0:T(8,128)} fusion(bf16[2,2,192,512]{3,2,0,1:T(8,128)(2,1)S(1)} %get-tuple-element.258, f32[1,2,2,192,128]{4,3,2,1,0:T(8,128)} %get-tuple-element.274, f32[2,2,192]{2,1,0:T(2,128)S(1)} %copy.59, pred[]{:T(512)S(6)} %compare.4, bf16[1536,128]{1,0:T(8,128)(2,1)S(1)} %get-tuple-element.288, s32[]{:T(128)S(6)} %select_n.25), kind=kOutput, calls=%fused_computation.7.clone.1 | convolution fusion | flops 100958208 | bytes 1708037 | tf_op jit(solution)/shard_map/while/body/eval_jaxpr/agcqr,rae->agcqe/dot_general | solution.py:49
  34.5 1.3 %broadcast_divide_fusion = f32[1,2,2,192,128]{4,3,2,1,0:T(8,128)S(1)} fusion(f32[1,2,2,192,128]{4,3,2,1,0:T(8,128)} %get-tuple-element.135, f32[2,2,192]{2,1,0:T(2,128)S(1)} %copy.41), kind=kLoop, calls=%fused_computation.35 | loop fusion | flops 98304 | bytes 789504 | tf_op jit(solution)/shard_map/div | solution.py:662
  36.2 0.5 collective-permute-start.4
  36.9 5.1 %shard_map.155 = bf16[48,1024]{1,0:T(8,128)(2,1)S(1)} custom-call(bf16[192,256]{1,0:T(8,128)(2,1)S(1)} %bitcast.105), custom_call_target="tpu_custom_call" | custom-call | bytes 5000000 | tf_op jit(solution)/shard_map/pallas_call | solution.py:366
  42.3 3.3 %fusion.12 = (f32[48]{0:T(128)S(1)}, bf16[48,2048]{1,0:T(8,128)(2,1)S(1)}) fusion(bf16[48,1024]{1,0:T(8,128)(2,1)S(1)} %shard_map.155, bf16[1024,2048]{1,0:T(8,128)(2,1)} %param.23, bf16[48,2048]{1,0:T(8,128)(2,1)} %param.24), kind=kOutput, calls=%fused_computation.26 | convolution fusion | flops 201916368 | bytes 4686016 | tf_op jit(solution)/shard_map/dot_general | solution.py:671
  45.8 72.2 %shard_map.156 = bf16[48,2048]{1,0:T(8,128)(2,1)S(1)} custom-call(bf16[48,2048]{1,0:T(8,128)(2,1)S(1)} %fusion.14.refs_0_, bf16[48,2048]{1,0:T(8,128)(2,1)S(1)} %get-tuple-element.204.refs_1_, f32[8,48,1]{2,1,0:T(8,128)S(1)} %copy.44.refs_2_, bf16[2048,256]{1,0:T(8,128)(2,1)S(1)} %bitcast.107, bf16[2048,256]{1,0:T(8,128)(2,1)S(1)} %collective-permute-done.refs_4_, ...), custom_call_target="tpu_custom_call" | custom-call | flops 7247757312 | bytes 30000000 | tf_op jit(solution)/shard_map/pallas_call | solution.py:552
  118.0 0.7 copy.73
  (67 shorter events, 1.6 us)
Async XLA Ops:
  0.0 5.0 %copy-start = (s32[192,4]{0,1:T(4,128)S(1)}, s32[192,4]{0,1:T(4,128)}, u32[]{:S(2)}) copy-start(s32[192,4]{0,1:T(4,128)} %param.26) | copy-start | bytes 9220
  0.0 36.7 %collective-permute-start.6 = (bf16[256,2048]{1,0:T(8,128)(2,1)}, bf16[256,2048]{1,0:T(8,128)(2,1)}, u32[]{:S(2)}, u32[]{:S(2)}) collective-permute-start(bf16[256,2048]{1,0:T(8,128)(2,1)} %bitcast.118), channel_id=1, source_target_pairs={{0,2},{1,3},{2,0},{3,1},{4,6},{5,7},{6,4},{7,5},{8,10},{9,11},{10,... | collective-permute-start | bytes 3145736 | tf_op jit(solution)/shard_map/ppermute | solution.py:620
  3.0 42.7 %collective-permute-start.5 = (bf16[256,2048]{1,0:T(8,128)(2,1)}, bf16[256,2048]{1,0:T(8,128)(2,1)}, u32[]{:S(2)}, u32[]{:S(2)}) collective-permute-start(bf16[256,2048]{1,0:T(8,128)(2,1)} %bitcast.119), channel_id=1, source_target_pairs={{0,1},{1,0},{2,3},{3,2},{4,5},{5,4},{6,7},{7,6},{8,9},{9,8},{10,11... | collective-permute-start | bytes 3145736 | tf_op jit(solution)/shard_map/ppermute | solution.py:620
  3.0 33.1 %collective-permute-start = (bf16[2048,256]{1,0:T(8,128)(2,1)}, bf16[2048,256]{1,0:T(8,128)(2,1)S(1)}, u32[]{:S(2)}, u32[]{:S(2)}) collective-permute-start(bf16[2048,256]{1,0:T(8,128)(2,1)} %bitcast.106), channel_id=1, source_target_pairs={{0,1},{1,0},{2,3},{3,2},{4,5},{5,4},{6,7},{7,6},{8,9},{9,8},{10,11... | collective-permute-start | bytes 3145736 | tf_op jit(solution)/shard_map/ppermute | solution.py:620
  3.5 32.7 %collective-permute-start.1 = (bf16[2048,256]{1,0:T(8,128)(2,1)}, bf16[2048,256]{1,0:T(8,128)(2,1)}, u32[]{:S(2)}, u32[]{:S(2)}) collective-permute-start(bf16[2048,256]{1,0:T(8,128)(2,1)} %bitcast.108), channel_id=1, source_target_pairs={{0,1},{1,0},{2,3},{3,2},{4,5},{5,4},{6,7},{7,6},{8,9},{9,8},{10,11... | collective-permute-start | bytes 3145736 | tf_op jit(solution)/shard_map/ppermute | solution.py:620
  3.5 42.2 %collective-permute-start.2 = (bf16[2048,256]{1,0:T(8,128)(2,1)}, bf16[2048,256]{1,0:T(8,128)(2,1)}, u32[]{:S(2)}, u32[]{:S(2)}) collective-permute-start(bf16[2048,256]{1,0:T(8,128)(2,1)} %refs_7_.1), channel_id=1, source_target_pairs={{0,1},{1,0},{2,3},{3,2},{4,5},{5,4},{6,7},{7,6},{8,9},{9,8},{10,11... | collective-permute-start | bytes 3145736 | tf_op jit(solution)/shard_map/ppermute | solution.py:620
  5.8 0.8 copy-start.1
  6.6 0.8 copy-start.2
  25.5 10.3 %copy-start.9 = (f32[2]{0:T(128)S(1)}, f32[2]{0:T(128)}, u32[]{:S(2)}) copy-start(f32[2]{0:T(128)} %param.21) | copy-start | bytes 28
  25.5 10.5 %copy-start.10 = (f32[128]{0:T(128)S(1)}, f32[128]{0:T(128)}, u32[]{:S(2)}) copy-start(f32[128]{0:T(128)} %param.22) | copy-start | bytes 1540
  25.5 10.7 %copy-start.7 = (bf16[256,2048]{1,0:T(8,128)(2,1)S(1)}, bf16[256,2048]{1,0:T(8,128)(2,1)}, u32[]{:S(2)}) copy-start(bf16[256,2048]{1,0:T(8,128)(2,1)} %refs_11_.1) | copy-start | bytes 3145732
  34.5 1.7 %copy-start.6 = (bf16[2048,256]{1,0:T(8,128)(2,1)S(1)}, bf16[2048,256]{1,0:T(8,128)(2,1)}, u32[]{:S(2)}) copy-start(bf16[2048,256]{1,0:T(8,128)(2,1)} %refs_9_.1) | copy-start | bytes 3145732
  36.1 9.6 %collective-permute-start.3 = (bf16[2048,256]{1,0:T(8,128)(2,1)S(1)}, bf16[2048,256]{1,0:T(8,128)(2,1)}, u32[]{:S(2)}, u32[]{:S(2)}) collective-permute-start(bf16[2048,256]{1,0:T(8,128)(2,1)S(1)} %copy-done.6), channel_id=1, source_target_pairs={{0,1},{1,0},{2,3},{3,2},{4,5},{5,4},{6,7},{7,6},{8,9},{9,8},{10,11... | collective-permute-start | bytes 3145736 | tf_op jit(solution)/shard_map/ppermute | solution.py:620
  36.2 9.5 %collective-permute-start.4 = (bf16[256,2048]{1,0:T(8,128)(2,1)S(1)}, bf16[256,2048]{1,0:T(8,128)(2,1)}, u32[]{:S(2)}, u32[]{:S(2)}) collective-permute-start(bf16[256,2048]{1,0:T(8,128)(2,1)S(1)} %copy-done.7), channel_id=1, source_target_pairs={{0,1},{1,0},{2,3},{3,2},{4,5},{5,4},{6,7},{7,6},{8,9},{9,8},{10,11... | collective-permute-start | bytes 3145736 | tf_op jit(solution)/shard_map/ppermute | solution.py:620
  36.7 9.1 %collective-permute-start.7 = (bf16[256,2048]{1,0:T(8,128)(2,1)}, bf16[256,2048]{1,0:T(8,128)(2,1)}, u32[]{:S(2)}, u32[]{:S(2)}) collective-permute-start(bf16[256,2048]{1,0:T(8,128)(2,1)} %collective-permute-done.6.refs_15_), channel_id=1, source_target_pairs={{0,1},{1,0},{2,3},{3,2},{4,5},{5,4},{6,7},{7,6},{8,9},{9,8},{10,11... | collective-permute-start | bytes 3145736 | tf_op jit(solution)/shard_map/ppermute | solution.py:620
  42.2 3.4 %copy-start.8 = (f32[2048]{0:T(1024)S(1)}, f32[2048]{0:T(1024)}, u32[]{:S(2)}) copy-start(f32[2048]{0:T(1024)} %param.25) | copy-start | bytes 24580
  42.2 3.6 %copy-start.3 = (bf16[1,2048,256]{2,1,0:T(8,128)(2,1)S(1)}, bf16[1,2048,256]{2,1,0:T(8,128)(2,1)}, u32[]{:S(2)}) copy-start(bf16[1,2048,256]{2,1,0:T(8,128)(2,1)} %param.28) | copy-start | bytes 3145732
  42.2 3.6 %copy-start.4 = (bf16[1,2048,256]{2,1,0:T(8,128)(2,1)S(1)}, bf16[1,2048,256]{2,1,0:T(8,128)(2,1)}, u32[]{:S(2)}) copy-start(bf16[1,2048,256]{2,1,0:T(8,128)(2,1)} %param.29) | copy-start | bytes 3145732
  42.3 3.5 %copy-start.5 = (bf16[2048,256]{1,0:T(8,128)(2,1)S(1)}, bf16[2048,256]{1,0:T(8,128)(2,1)}, u32[]{:S(2)}) copy-start(bf16[2048,256]{1,0:T(8,128)(2,1)} %refs_7_.1) | copy-start | bytes 3145732
where the time goes:
time: 119 us
  Pallas kernels  95.4 us (80%)
  matrix products  10.3 us (9%)
  starting transfers between devices  4.66 us (4%)
  local copies, waits for them, and re-layouts  4.07 us (3%)
  other arithmetic  3.86 us (3%)
    pallas_call x1, Pallas kernels, run_moe(): pl.pallas_call(partial(moe_kernel, sp), out_shape=jax.ShapeDtypeStruct((c...  72.2 us
    pallas_call x1, Pallas kernels, gather_sp(): pl.pallas_call(partial(gather_kernel, sp, tp, count, with_tp), out_shape=...  18 us
    dot_general x3, matrix products, attention_block(): jnp.einsum('agcqr,rae->agcqe', weights.astype(jnp.bfloat16), value_heads,...  5.41 us
    pallas_call x1, Pallas kernels, exchange_heads(): pl.pallas_call(partial(heads_kernel, tp), out_shape=jax.ShapeDtypeStruct(...  5.13 us
    ppermute x8, starting transfers between devices, swapped(): return lax.ppermute(array, 'tp', [(i, i ^ step) for i in range(tp)])  4.66 us
    unnamed x26, local copies, waits for them, and re-layouts  3.34 us
    dot_general x1, matrix products, dense_body(): jnp.dot(attended, out_weight, preferred_element_type=jnp.float32)  3.31 us
  transfers between devices with their start and end apart: 8, of which 0 were waited for; matrix products, arithmetic and copies ran while one was open for 13% of the time, Pallas kernels for 20%

commit v1 on v0

--- a/solution.py
+++ b/solution.py
@@ -387,8 +387,8 @@
     sources = refs[3:17]
     out_ref = refs[17]
     gate, up, down, sgate, sup, sdown = refs[18:24]
-    rows, hid_own, hid_out, hid_in, parts, xin, zout, zin, sout, sin = refs[24:34]
-    zs, zr, xs, xr, ys, yr, hs, hr, os_, or_, rs, rr, ss, sr, wsem = refs[34:]
+    rows, hid_own, hid_out, hid_in, parts, xin, zout, zin, sout, sin, total = refs[24:35]
+    zs, zr, xs, xr, ys, yr, hs, hr, os_, or_, rs, rr, ss, sr, wsem = refs[35:]
     s, t, z, x, depth = grid_place(sp)
     count, width = normed_ref.shape
     quarter = sources[0].shape[1]
@@ -417,125 +417,140 @@
         load.start()
     peer_barrier(line + [across, mirror])
 
-    z_rows, x_rows, y_rows, hids, x_outs, z_outs = {}, {}, {}, {}, {}, {}
-
-    def send_y(j, xx, source):
-        y_rows[j, xx] = remote(
-            source, rows.at[1, j, xx], ys.at[2 * j + xx], yr.at[2 * j + xx], mirror
-        )
-        y_rows[j, xx].start()
-
-    def send_x(j, source):
-        x_rows[j] = remote(source, rows.at[0, j, 1], xs.at[j], xr.at[j], across)
-        x_rows[j].start()
-
-    order = [0, 1, 3, 2] if depth == 4 else list(range(depth))
-    send_y(0, 0, normed_ref)
-    send_x(0, normed_ref)
-    for j in order[1:]:
-        k = depth - j
-        z_rows[j] = remote(
-            normed_ref, rows.at[0, j, 0], zs.at[k - 1], zr.at[k - 1], line[k - 1]
-        )
-        z_rows[j].start()
-    rows[0, 0, 0] = normed_ref[...]
+    z_rows, started = {}, []
+    x_rows, y_rows, diagonal, hids, x_outs, z_outs = {}, {}, {}, {}, {}, {}
+
+    def send(source, target, send_sem, recv_sem, peer):
+        copy = remote(source, target, send_sem, recv_sem, peer)
+        copy.start()
+        started.append(copy)
+        return copy
+
+    def own_rows(j):
+        return normed_ref if j == 0 else rows.at[0, j, 0]
 
     def hidden_of(block, gate_buf, up_buf):
         gate_value = jnp.dot(block, gate_buf[...], preferred_element_type=jnp.float32)
         up_value = jnp.dot(block, up_buf[...], preferred_element_type=jnp.float32)
         return (jax.nn.silu(gate_value) * up_value).astype(jnp.bfloat16)
 
-    def relay(j):
-        if j == 0:
-            return
-        z_rows[j].wait_recv()
-        send_x(j, rows.at[0, j, 0])
-        send_y(j, 0, rows.at[0, j, 0])
-
-    def own_plane(j):
-        x_rows[j].wait_recv()
-        send_y(j, 1, rows.at[0, j, 1])
-        if j == 0:
-            for load in loads[:4]:
-                load.wait()
+    waited = set()
+
+    def arrived(copies, j):
+        if (id(copies), j) not in waited:
+            waited.add((id(copies), j))
+            copies[j].wait_recv()
+
+    def loaded(first_load, last_load):
+        for n in range(first_load, last_load):
+            if ("load", n) not in waited:
+                waited.add(("load", n))
+                loads[n].wait()
+
+    def RX(j):
+        if j != 0:
+            arrived(z_rows, j)
+        x_rows[j] = send(own_rows(j), rows.at[0, j, 1], xs.at[j], xr.at[j], across)
+
+    def RY(j):
+        if j != 0:
+            arrived(z_rows, j)
+        y_rows[j] = send(own_rows(j), rows.at[1, j, 0], ys.at[j], yr.at[j], mirror)
+
+    def RD(j):
+        sems = ys.at[depth + j], yr.at[depth + j]
+        if j in by_x:
+            arrived(y_rows, j)
+            diagonal[j] = send(rows.at[1, j, 0], rows.at[1, j, 1], *sems, across)
+        else:
+            arrived(x_rows, j)
+            diagonal[j] = send(rows.at[0, j, 1], rows.at[1, j, 1], *sems, mirror)
+
+    def HO(j):
+        arrived(x_rows, j)
+        loaded(0, 4)
         hid_own[j] = hidden_of(rows[0, j].reshape(2 * count, width), gate, up)
 
-    def other_plane(j):
-        if j != 0:
-            y_rows[j, 0].wait_recv()
-        y_rows[j, 1].wait_recv()
+    def HP(j):
+        arrived(y_rows, j)
+        arrived(diagonal, j)
+        loaded(0, 4)
         hid_out[j] = hidden_of(rows[1, j].reshape(2 * count, width), gate, up)
-        hids[j] = remote(hid_out.at[j], hid_in.at[j], hs.at[j], hr.at[j], mirror)
-        hids[j].start()
-
-    def finish_down(j):
-        if j == 0:
-            for load in loads[10:]:
-                load.wait()
-        hids[j].wait_recv()
+        hids[j] = send(hid_out.at[j], hid_in.at[j], hs.at[j], hr.at[j], mirror)
+
+    def FD(j):
+        loaded(10, 14)
+        arrived(hids, j)
         half = hid_own.shape[2]
         value = jnp.dot(
             hid_own[j], down[pl.ds(0, half)], preferred_element_type=jnp.float32
         ) + jnp.dot(hid_in[j], down[pl.ds(half, half)], preferred_element_type=jnp.float32)
         base = lax.rem(z + j, depth) * 2
         parts[j, 1] = (value[count:] * weight_ref[base + 1 - x]).astype(jnp.bfloat16)
-        x_outs[j] = remote(parts.at[j, 1], xin.at[j], os_.at[j], or_.at[j], across)
-        x_outs[j].start()
+        x_outs[j] = send(parts.at[j, 1], xin.at[j], os_.at[j], or_.at[j], across)
         parts[j, 0] = (value[:count] * weight_ref[base + x]).astype(jnp.bfloat16)
 
-    def fold(j):
-        x_outs[j].wait_recv()
-        if j == 0:
-            return
+    def FO(j):
+        arrived(x_outs, j)
         zout[j - 1] = (parts[j, 0].astype(jnp.float32) + xin[j].astype(jnp.float32)).astype(
             jnp.bfloat16
         )
-        z_outs[j] = remote(
+        z_outs[j] = send(
             zout.at[j - 1], zin.at[j - 1], rs.at[j - 1], rr.at[j - 1], line[j - 1]
         )
-        z_outs[j].start()
-
-    relay(order[1])
-    own_plane(order[0])
-    y_rows[0, 0].wait_recv()
-    for load in loads[4:10]:
-        load.wait()
-    pair = jnp.concatenate([normed_ref[...], rows[1, 0, 0]], axis=0)
-    shared = jnp.dot(
-        hidden_of(pair, sgate, sup), sdown[...], preferred_element_type=jnp.float32
-    )
-    sout[...] = shared[count:].astype(jnp.bfloat16)
-    shared_copy = remote(sout, sin, ss, sr, mirror)
-    shared_copy.start()
-    total = stream_ref[...].astype(jnp.float32) + shared[:count]
-    relay(order[2])
-    own_plane(order[1])
-    other_plane(order[0])
-    relay(order[3])
-    own_plane(order[2])
-    other_plane(order[1])
-    finish_down(order[0])
-    own_plane(order[3])
-    other_plane(order[2])
-    finish_down(order[1])
-    fold(order[0])
-    other_plane(order[3])
-    finish_down(order[2])
-    fold(order[1])
-    finish_down(order[3])
-    fold(order[2])
-    fold(order[3])
-    shared_copy.wait_recv()
-    total = total + sin[...].astype(jnp.float32)
-    total = total + parts[0, 0].astype(jnp.float32) + xin[0].astype(jnp.float32)
-    for j in order[1:]:
-        z_outs[j].wait_recv()
-        total = total + zin[j - 1].astype(jnp.float32)
-    out_ref[...] = total.astype(out_ref.dtype)
-    for group in (z_rows, x_rows, y_rows, hids, x_outs, z_outs):
-        for copy in group.values():
-            copy.wait_send()
-    shared_copy.wait_send()
+
+    shared_copy = []
+
+    def SH(j):
+        arrived(y_rows, 0)
+        loaded(4, 10)
+        pair = jnp.concatenate([normed_ref[...], rows[1, 0, 0]], axis=0)
+        shared = jnp.dot(
+            hidden_of(pair, sgate, sup), sdown[...], preferred_element_type=jnp.float32
+        )
+        sout[...] = shared[count:].astype(jnp.bfloat16)
+        total[...] = stream_ref[...].astype(jnp.float32) + shared[:count]
+
+    def SS(j):
+        shared_copy.append(send(sout, sin, ss, sr, mirror))
+
+    actions = {f.__name__: f for f in (RX, RY, RD, HO, HP, FD, FO, SH, SS)}
+    by_x, steps = moe_plan()
+    rows[0, 0, 0] = normed_ref[...]
+    for j in [1, 3, 2] if depth == 4 else range(1, depth):
+        k = depth - j
+        z_rows[j] = send(
+            normed_ref, rows.at[0, j, 0], zs.at[k - 1], zr.at[k - 1], line[k - 1]
+        )
+    for step in steps:
+        actions[step[:2]](int(step[2:] or 0))
+    shared_copy[0].wait_recv()
+    arrived(x_outs, 0)
+    value = total[...] + sin[...].astype(jnp.float32)
+    value = value + parts[0, 0].astype(jnp.float32) + xin[0].astype(jnp.float32)
+    for j in range(1, depth):
+        arrived(z_outs, j)
+        value = value + zin[j - 1].astype(jnp.float32)
+    out_ref[...] = value.astype(out_ref.dtype)
+    for copy in started:
+        copy.wait_send()
+
+
+def moe_plan():
+    return (0, 3), [
+        step
+        for group in (
+            "RY0 RX0 RY1 RX1",
+            "RY3 RX3 HO1 RD1",
+            "RX2 RY2 RD3 HP1",
+            "RD0 RD2 HO3 HP3",
+            "FD1 HP2 FD3 FO1",
+            "HP0 HO2 FD2 FO3",
+            "HO0 FD0 FO2 SH",
+            "SS",
+        )
+        for step in group.split()
+    ]
 
 
 def run_moe(normed, stream, weights, sources, sp, collective_id):
@@ -571,6 +586,7 @@
             pltpu.VMEM((depth - 1, count, width), bf16),
             pltpu.VMEM((count, width), bf16),
             pltpu.VMEM((count, width), bf16),
+            pltpu.VMEM((count, width), jnp.float32),
         ]
         + dma(depth - 1)
         + dma(depth)

time: 119 us -> 106 us (0.89)
  Pallas kernels: 95.4 us -> 82.8 us
    pallas_call x1, Pallas kernels: 72.2 us -> 59.6 us  [run_moe(): pl.pallas_call(partial(moe_kernel, sp), out_shape=jax.ShapeDtypeStruct((c...]
  transfers between devices with their start and end apart: 8 -> 8, of which waited for: 0 -> 0; matrix products, arithmetic and copies ran while one was open for 13% -> 15% of each run, Pallas kernels for 20% -> 22%
where the time goes in v1:
time: 106 us
  Pallas kernels  82.8 us (78%)
  matrix products  10.3 us (10%)
  starting transfers between devices  4.66 us (4%)
  local copies, waits for them, and re-layouts  4.07 us (4%)
  other arithmetic  3.86 us (4%)
    pallas_call x1, Pallas kernels, run_moe(): pl.pallas_call(partial(moe_kernel, sp), out_shape=jax.ShapeDtypeStruct((c...  59.6 us
    pallas_call x1, Pallas kernels, gather_sp(): pl.pallas_call(partial(gather_kernel, sp, tp, count, with_tp), out_shape=...  18 us
    dot_general x3, matrix products, attention_block(): jnp.einsum('agcqr,rae->agcqe', weights.astype(jnp.bfloat16), value_heads,...  5.41 us
    pallas_call x1, Pallas kernels, exchange_heads(): pl.pallas_call(partial(heads_kernel, tp), out_shape=jax.ShapeDtypeStruct(...  5.13 us
    ppermute x8, starting transfers between devices, swapped(): return lax.ppermute(array, 'tp', [(i, i ^ step) for i in range(tp)])  4.66 us
    unnamed x26, local copies, waits for them, and re-layouts  3.34 us
    dot_general x1, matrix products, dense_body(): jnp.dot(attended, out_weight, preferred_element_type=jnp.float32)  3.31 us
  transfers between devices with their start and end apart: 8, of which 0 were waited for; matrix products, arithmetic and copies ran while one was open for 15% of the time, Pallas kernels for 22%

profile of v1, /device:TPU:0, one launch (start us, length us, event | category | flops | bytes accessed | tf_op | source)
XLA Modules:
  0.0 106.1 jit_solution(11761760171251874483)
XLA Ops:
  0.0 3.0 %collective-permute-start.6 = (bf16[256,2048]{1,0:T(8,128)(2,1)}, bf16[256,2048]{1,0:T(8,128)(2,1)}, u32[]{:S(2)}, u32[]{:S(2)}) collective-permute-start(bf16[256,2048]{1,0:T(8,128)(2,1)} %bitcast.118), channel_id=1, source_target_pairs={{0,2},{1,3},{2,0},{3,1},{4,6},{5,7},{6,4},{7,5},{8,10},{9,11},{10,... | collective-permute-start | bytes 3145736 | tf_op jit(solution)/shard_map/ppermute | solution.py:636
  3.0 0.5 collective-permute-start
  3.5 0.5 collective-permute-start.2
  4.0 1.0 copy.38
  5.1 0.7 select_reduce_fusion
  5.8 0.8 copy-done.1
  6.6 0.8 copy-done.2
  7.4 18.0 %shard_map.154 = (bf16[8,192,128]{2,1,0:T(8,128)(2,1)S(1)}, bf16[8,192,128]{2,1,0:T(8,128)(2,1)S(1)}, f32[8,8,128]{2,1,0:T(8,128)S(1)}) custom-call(bf16[192,128]{1,0:T(8,128)(2,1)S(1)} %copy-done.1, bf16[192,128]{1,0:T(8,128)(2,1)S(1)} %copy-done.2, f32[8,128]{1,0:T(8,128)S(1)} %pad.4.refs_2_), custom_call_target="tpu_custom_call" | custom-call | bytes 40000000 | tf_op jit(solution)/shard_map/pallas_call | solution.py:317
  25.5 9.0 %while.18 = (s32[]{:T(128)}, f32[1,2,2,192]{3,1,2,0:T(2,128)S(1)}, f32[1,2,2,192]{3,1,2,0:T(2,128)S(1)}, f32[1,2,2,192,128]{4,3,2,1,0:T(8,128)}, bf16[1536,128]{...) while((s32[]{:T(128)}, f32[1,2,2,192]{3,1,2,0:T(2,128)S(1)}, ...), condition=%wide.region_4.5_spmd.clone, body=%wide.region_1.4_spmd.clone.sunk | while | flops 153260544 | bytes 6443191 | solution.py:78
  25.7 0.5 bitcast_reduce_fusion.2
  26.2 0.4 fusion.31
  26.7 1.1 %fusion.32 = f32[1,2,2,192,128]{4,3,2,1,0:T(8,128)} fusion(bf16[2,2,192,512]{3,2,0,1:T(8,128)(2,1)S(1)} %get-tuple-element.258, f32[1,2,2,192,128]{4,3,2,1,0:T(8,128)} %get-tuple-element.274, f32[2,2,192]{2,1,0:T(2,128)S(1)} %copy.59, pred[]{:T(512)S(6)} %compare.4, bf16[1536,128]{1,0:T(8,128)(2,1)S(1)} %get-tuple-element.288, s32[]{:T(128)S(6)} %select_n.25), kind=kOutput, calls=%fused_computation.7.clone.1 | convolution fusion | flops 100958208 | bytes 1708037 | tf_op jit(solution)/shard_map/while/body/eval_jaxpr/agcqr,rae->agcqe/dot_general | solution.py:49
  28.0 0.5 bitcast_reduce_fusion.2
  28.5 0.4 fusion.31
  29.0 2.1 %fusion.32 = f32[1,2,2,192,128]{4,3,2,1,0:T(8,128)} fusion(bf16[2,2,192,512]{3,2,0,1:T(8,128)(2,1)S(1)} %get-tuple-element.258, f32[1,2,2,192,128]{4,3,2,1,0:T(8,128)} %get-tuple-element.274, f32[2,2,192]{2,1,0:T(2,128)S(1)} %copy.59, pred[]{:T(512)S(6)} %compare.4, bf16[1536,128]{1,0:T(8,128)(2,1)S(1)} %get-tuple-element.288, s32[]{:T(128)S(6)} %select_n.25), kind=kOutput, calls=%fused_computation.7.clone.1 | convolution fusion | flops 100958208 | bytes 1708037 | tf_op jit(solution)/shard_map/while/body/eval_jaxpr/agcqr,rae->agcqe/dot_general | solution.py:49
  31.3 0.5 bitcast_reduce_fusion.2
  31.8 0.4 fusion.31
  32.3 2.1 %fusion.32 = f32[1,2,2,192,128]{4,3,2,1,0:T(8,128)} fusion(bf16[2,2,192,512]{3,2,0,1:T(8,128)(2,1)S(1)} %get-tuple-element.258, f32[1,2,2,192,128]{4,3,2,1,0:T(8,128)} %get-tuple-element.274, f32[2,2,192]{2,1,0:T(2,128)S(1)} %copy.59, pred[]{:T(512)S(6)} %compare.4, bf16[1536,128]{1,0:T(8,128)(2,1)S(1)} %get-tuple-element.288, s32[]{:T(128)S(6)} %select_n.25), kind=kOutput, calls=%fused_computation.7.clone.1 | convolution fusion | flops 100958208 | bytes 1708037 | tf_op jit(solution)/shard_map/while/body/eval_jaxpr/agcqr,rae->agcqe/dot_general | solution.py:49
  34.5 1.3 %broadcast_divide_fusion = f32[1,2,2,192,128]{4,3,2,1,0:T(8,128)S(1)} fusion(f32[1,2,2,192,128]{4,3,2,1,0:T(8,128)} %get-tuple-element.135, f32[2,2,192]{2,1,0:T(2,128)S(1)} %copy.41), kind=kLoop, calls=%fused_computation.35 | loop fusion | flops 98304 | bytes 789504 | tf_op jit(solution)/shard_map/div | solution.py:678
  36.2 0.5 collective-permute-start.4
  36.9 5.1 %shard_map.155 = bf16[48,1024]{1,0:T(8,128)(2,1)S(1)} custom-call(bf16[192,256]{1,0:T(8,128)(2,1)S(1)} %bitcast.105), custom_call_target="tpu_custom_call" | custom-call | bytes 5000000 | tf_op jit(solution)/shard_map/pallas_call | solution.py:366
  42.3 3.3 %fusion.12 = (f32[48]{0:T(128)S(1)}, bf16[48,2048]{1,0:T(8,128)(2,1)S(1)}) fusion(bf16[48,1024]{1,0:T(8,128)(2,1)S(1)} %shard_map.155, bf16[1024,2048]{1,0:T(8,128)(2,1)} %param.23, bf16[48,2048]{1,0:T(8,128)(2,1)} %param.24), kind=kOutput, calls=%fused_computation.26 | convolution fusion | flops 201916368 | bytes 4686016 | tf_op jit(solution)/shard_map/dot_general | solution.py:687
  45.8 59.6 %shard_map.156 = bf16[48,2048]{1,0:T(8,128)(2,1)S(1)} custom-call(bf16[48,2048]{1,0:T(8,128)(2,1)S(1)} %fusion.14.refs_0_, bf16[48,2048]{1,0:T(8,128)(2,1)S(1)} %get-tuple-element.204.refs_1_, f32[8,48,1]{2,1,0:T(8,128)S(1)} %copy.44.refs_2_, bf16[2048,256]{1,0:T(8,128)(2,1)S(1)} %bitcast.107, bf16[2048,256]{1,0:T(8,128)(2,1)S(1)} %collective-permute-done.refs_4_, ...), custom_call_target="tpu_custom_call" | custom-call | flops 7247757312 | bytes 30000000 | tf_op jit(solution)/shard_map/pallas_call | solution.py:567
  105.4 0.7 copy.73
  (67 shorter events, 1.6 us)
Async XLA Ops:
  0.0 5.0 %copy-start = (s32[192,4]{0,1:T(4,128)S(1)}, s32[192,4]{0,1:T(4,128)}, u32[]{:S(2)}) copy-start(s32[192,4]{0,1:T(4,128)} %param.26) | copy-start | bytes 9220
  0.0 36.7 %collective-permute-start.6 = (bf16[256,2048]{1,0:T(8,128)(2,1)}, bf16[256,2048]{1,0:T(8,128)(2,1)}, u32[]{:S(2)}, u32[]{:S(2)}) collective-permute-start(bf16[256,2048]{1,0:T(8,128)(2,1)} %bitcast.118), channel_id=1, source_target_pairs={{0,2},{1,3},{2,0},{3,1},{4,6},{5,7},{6,4},{7,5},{8,10},{9,11},{10,... | collective-permute-start | bytes 3145736 | tf_op jit(solution)/shard_map/ppermute | solution.py:636
  3.0 42.7 %collective-permute-start.5 = (bf16[256,2048]{1,0:T(8,128)(2,1)}, bf16[256,2048]{1,0:T(8,128)(2,1)}, u32[]{:S(2)}, u32[]{:S(2)}) collective-permute-start(bf16[256,2048]{1,0:T(8,128)(2,1)} %bitcast.119), channel_id=1, source_target_pairs={{0,1},{1,0},{2,3},{3,2},{4,5},{5,4},{6,7},{7,6},{8,9},{9,8},{10,11... | collective-permute-start | bytes 3145736 | tf_op jit(solution)/shard_map/ppermute | solution.py:636
  3.0 33.1 %collective-permute-start = (bf16[2048,256]{1,0:T(8,128)(2,1)}, bf16[2048,256]{1,0:T(8,128)(2,1)S(1)}, u32[]{:S(2)}, u32[]{:S(2)}) collective-permute-start(bf16[2048,256]{1,0:T(8,128)(2,1)} %bitcast.106), channel_id=1, source_target_pairs={{0,1},{1,0},{2,3},{3,2},{4,5},{5,4},{6,7},{7,6},{8,9},{9,8},{10,11... | collective-permute-start | bytes 3145736 | tf_op jit(solution)/shard_map/ppermute | solution.py:636
  3.5 32.7 %collective-permute-start.1 = (bf16[2048,256]{1,0:T(8,128)(2,1)}, bf16[2048,256]{1,0:T(8,128)(2,1)}, u32[]{:S(2)}, u32[]{:S(2)}) collective-permute-start(bf16[2048,256]{1,0:T(8,128)(2,1)} %bitcast.108), channel_id=1, source_target_pairs={{0,1},{1,0},{2,3},{3,2},{4,5},{5,4},{6,7},{7,6},{8,9},{9,8},{10,11... | collective-permute-start | bytes 3145736 | tf_op jit(solution)/shard_map/ppermute | solution.py:636
  3.5 42.2 %collective-permute-start.2 = (bf16[2048,256]{1,0:T(8,128)(2,1)}, bf16[2048,256]{1,0:T(8,128)(2,1)}, u32[]{:S(2)}, u32[]{:S(2)}) collective-permute-start(bf16[2048,256]{1,0:T(8,128)(2,1)} %refs_7_.1), channel_id=1, source_target_pairs={{0,1},{1,0},{2,3},{3,2},{4,5},{5,4},{6,7},{7,6},{8,9},{9,8},{10,11... | collective-permute-start | bytes 3145736 | tf_op jit(solution)/shard_map/ppermute | solution.py:636
  5.8 0.8 copy-start.1
  6.6 0.8 copy-start.2
  25.5 10.3 %copy-start.9 = (f32[2]{0:T(128)S(1)}, f32[2]{0:T(128)}, u32[]{:S(2)}) copy-start(f32[2]{0:T(128)} %param.21) | copy-start | bytes 28
  25.5 10.5 %copy-start.10 = (f32[128]{0:T(128)S(1)}, f32[128]{0:T(128)}, u32[]{:S(2)}) copy-start(f32[128]{0:T(128)} %param.22) | copy-start | bytes 1540
  25.5 10.7 %copy-start.7 = (bf16[256,2048]{1,0:T(8,128)(2,1)S(1)}, bf16[256,2048]{1,0:T(8,128)(2,1)}, u32[]{:S(2)}) copy-start(bf16[256,2048]{1,0:T(8,128)(2,1)} %refs_11_.1) | copy-start | bytes 3145732
  34.5 1.7 %copy-start.6 = (bf16[2048,256]{1,0:T(8,128)(2,1)S(1)}, bf16[2048,256]{1,0:T(8,128)(2,1)}, u32[]{:S(2)}) copy-start(bf16[2048,256]{1,0:T(8,128)(2,1)} %refs_9_.1) | copy-start | bytes 3145732
  36.1 9.6 %collective-permute-start.3 = (bf16[2048,256]{1,0:T(8,128)(2,1)S(1)}, bf16[2048,256]{1,0:T(8,128)(2,1)}, u32[]{:S(2)}, u32[]{:S(2)}) collective-permute-start(bf16[2048,256]{1,0:T(8,128)(2,1)S(1)} %copy-done.6), channel_id=1, source_target_pairs={{0,1},{1,0},{2,3},{3,2},{4,5},{5,4},{6,7},{7,6},{8,9},{9,8},{10,11... | collective-permute-start | bytes 3145736 | tf_op jit(solution)/shard_map/ppermute | solution.py:636
  36.2 9.5 %collective-permute-start.4 = (bf16[256,2048]{1,0:T(8,128)(2,1)S(1)}, bf16[256,2048]{1,0:T(8,128)(2,1)}, u32[]{:S(2)}, u32[]{:S(2)}) collective-permute-start(bf16[256,2048]{1,0:T(8,128)(2,1)S(1)} %copy-done.7), channel_id=1, source_target_pairs={{0,1},{1,0},{2,3},{3,2},{4,5},{5,4},{6,7},{7,6},{8,9},{9,8},{10,11... | collective-permute-start | bytes 3145736 | tf_op jit(solution)/shard_map/ppermute | solution.py:636
  36.7 9.1 %collective-permute-start.7 = (bf16[256,2048]{1,0:T(8,128)(2,1)}, bf16[256,2048]{1,0:T(8,128)(2,1)}, u32[]{:S(2)}, u32[]{:S(2)}) collective-permute-start(bf16[256,2048]{1,0:T(8,128)(2,1)} %collective-permute-done.6.refs_15_), channel_id=1, source_target_pairs={{0,1},{1,0},{2,3},{3,2},{4,5},{5,4},{6,7},{7,6},{8,9},{9,8},{10,11... | collective-permute-start | bytes 3145736 | tf_op jit(solution)/shard_map/ppermute | solution.py:636
  42.2 3.4 %copy-start.8 = (f32[2048]{0:T(1024)S(1)}, f32[2048]{0:T(1024)}, u32[]{:S(2)}) copy-start(f32[2048]{0:T(1024)} %param.25) | copy-start | bytes 24580
  42.2 3.6 %copy-start.3 = (bf16[1,2048,256]{2,1,0:T(8,128)(2,1)S(1)}, bf16[1,2048,256]{2,1,0:T(8,128)(2,1)}, u32[]{:S(2)}) copy-start(bf16[1,2048,256]{2,1,0:T(8,128)(2,1)} %param.28) | copy-start | bytes 3145732
  42.2 3.6 %copy-start.4 = (bf16[1,2048,256]{2,1,0:T(8,128)(2,1)S(1)}, bf16[1,2048,256]{2,1,0:T(8,128)(2,1)}, u32[]{:S(2)}) copy-start(bf16[1,2048,256]{2,1,0:T(8,128)(2,1)} %param.29) | copy-start | bytes 3145732
  42.3 3.5 %copy-start.5 = (bf16[2048,256]{1,0:T(8,128)(2,1)S(1)}, bf16[2048,256]{1,0:T(8,128)(2,1)}, u32[]{:S(2)}) copy-start(bf16[2048,256]{1,0:T(8,128)(2,1)} %refs_7_.1) | copy-start | bytes 3145732

commit v2 on v1

v2 whole, which is shorter than its diff:
```python
from functools import partial

import jax
import jax.numpy as jnp
from jax import lax
from jax.experimental import pallas as pl
from jax.experimental.pallas import tpu as pltpu
from jax.sharding import PartitionSpec as P

norm_eps = 1e-06
lowest_score = -1e30


def slot_targets(block_routes, experts, capacity):
    flat_routes = block_routes.reshape(-1)
    onehot = (flat_routes[:, None] == jnp.arange(experts, dtype=jnp.int32)[None, :]).astype(
        jnp.int32
    )
    earlier = jnp.cumsum(onehot, axis=0) - onehot
    return flat_routes * capacity + jnp.sum(earlier * onehot, axis=1)


def build_buffer(token_rows, block_routes, experts, capacity):
    targets = slot_targets(block_routes, experts, capacity)
    row_total = block_routes.shape[0]
    route_count = block_routes.shape[1]
    source_row = jnp.arange(row_total * route_count, dtype=jnp.int32) // route_count
    holder = jnp.full((experts * capacity,), row_total, jnp.int32).at[targets].set(source_row)
    padded = jnp.concatenate(
        [token_rows, jnp.zeros((1, token_rows.shape[1]), token_rows.dtype)], axis=0
    )
    return (padded[holder], targets)


def attention_block(carried, queries, key_block, value_block, score_scale):
    run_max, run_sum, accumulated = carried
    kv_local = run_max.shape[0]
    key_heads = key_block.reshape(key_block.shape[0], kv_local, 2, -1)
    value_heads = value_block.reshape(value_block.shape[0], kv_local, -1)
    scores = (
        jnp.einsum("qagcd,racd->agcqr", queries, key_heads, preferred_element_type=jnp.float32)
        * score_scale
    )
    new_max = jnp.maximum(run_max, jnp.max(scores, axis=-1))
    rescale = jnp.exp(run_max - new_max)
    weights = jnp.exp(scores - new_max[..., None])
    run_sum = run_sum * rescale + jnp.sum(weights, axis=-1)
    update = jnp.einsum(
        "agcqr,rae->agcqe",
        weights.astype(jnp.bfloat16),
        value_heads,
        preferred_element_type=jnp.float32,
    )
    return (new_max, run_sum, accumulated * rescale[..., None] + update)


def fold_keys(carried, pieces, first_row, queries, score_scale):
    key_piece, value_piece = pieces
    total_rows = key_piece.shape[0]
    block_rows = total_rows
    for candidate in (2048, 1024, 512):
        if total_rows % candidate == 0:
            block_rows = candidate
            break
    block_count = total_rows // block_rows

    def block_step(block_index, running):
        start_row = block_index * block_rows
        return attention_block(
            running,
            queries,
            lax.dynamic_slice_in_dim(key_piece, start_row, block_rows, 0),
            lax.dynamic_slice_in_dim(value_piece, start_row, block_rows, 0),
            score_scale,
        )

    return lax.fori_loop(0, block_count, block_step, carried)


def whole_experts(arrived, whole_gate, whole_up, whole_down, senders, capacity, groups):
    local_experts = whole_gate.shape[0]
    width = arrived.shape[-1]
    rows_in = arrived.reshape(senders, local_experts, capacity, width)
    gate_value = jnp.einsum(
        "sjtd,jdf->sjtf", rows_in, whole_gate, preferred_element_type=jnp.float32
    )
    up_value = jnp.einsum("sjtd,jdf->sjtf", rows_in, whole_up, preferred_element_type=jnp.float32)
    hidden = (jax.nn.silu(gate_value) * up_value).astype(jnp.bfloat16)
    hidden_units = hidden.shape[-1]
    hidden = hidden.reshape(senders, local_experts, capacity, groups, hidden_units // groups)
    down_groups = whole_down.reshape(local_experts, groups, hidden_units // groups, width)
    group_sums = jnp.einsum(
        "sjtgf,jgfd->sjtgd", hidden, down_groups, preferred_element_type=jnp.float32
    )
    group_sums = lax.optimization_barrier(group_sums.astype(jnp.bfloat16)).astype(jnp.float32)
    return (
        jnp.sum(group_sums, axis=3)
        .astype(jnp.bfloat16)
        .reshape(senders * local_experts * capacity, width)
    )


def body(
    query_maps,
    key_maps,
    value_rows,
    mix_lambda,
    head_gain,
    out_weight,
    residual,
    norm_gain,
    routes,
    route_weight,
    expert_gate,
    expert_up,
    expert_down,
    shared_gate,
    shared_up,
    shared_down,
):
    local_heads = mix_lambda.shape[0]
    head_width = head_gain.shape[0]
    kv_local = value_rows.shape[1] // head_width
    head_group = local_heads // kv_local
    head_dim = key_maps.shape[1] // (2 * kv_local)
    token_count = query_maps.shape[0]
    queries = query_maps.reshape(token_count, kv_local, head_group, 2, head_dim)
    start_max = jnp.full((kv_local, head_group, 2, token_count), lowest_score, jnp.float32)
    start_sum = jnp.zeros((kv_local, head_group, 2, token_count), jnp.float32)
    start_values = jnp.zeros((kv_local, head_group, 2, token_count, head_width), jnp.float32)
    folder = partial(fold_keys, queries=queries, score_scale=head_dim ** (-0.5))
    _, run_sum, accumulated = folder(
        (start_max, start_sum, start_values),
        (
            lax.all_gather(key_maps, "sp", axis=0, tiled=True),
            lax.all_gather(value_rows, "sp", axis=0, tiled=True),
        ),
        jnp.int32(0),
    )
    normalized = accumulated / run_sum[..., None]
    lambdas = mix_lambda.reshape(kv_local, head_group, 1, 1)
    difference = normalized[:, :, 0] - lambdas * normalized[:, :, 1]
    inverse_rms = lax.rsqrt(jnp.mean(difference * difference, axis=-1, keepdims=True) + norm_eps)
    head_scaled = (difference * inverse_rms * head_gain).astype(jnp.bfloat16)
    attended = jnp.transpose(head_scaled, (2, 0, 1, 3)).reshape(
        token_count, local_heads * head_width
    )
    columns = lax.axis_size("tp")
    column = lax.axis_index("tp")
    rows_dev = token_count // columns
    own_rows = lax.dynamic_slice_in_dim(
        out_weight, column * attended.shape[1], attended.shape[1], 0
    )
    projected = lax.psum_scatter(
        jnp.dot(attended, own_rows, preferred_element_type=jnp.float32).astype(jnp.bfloat16),
        "tp",
        scatter_dimension=0,
        tiled=True,
    ).astype(jnp.float32)
    stream = (residual.astype(jnp.float32) + projected).astype(jnp.bfloat16)
    stream_wide = stream.astype(jnp.float32)
    stream_rms = lax.rsqrt(jnp.mean(stream_wide * stream_wide, axis=1, keepdims=True) + norm_eps)
    normed = (stream_wide * stream_rms * norm_gain).astype(jnp.bfloat16)
    senders = lax.axis_size("sp")
    local_experts = expert_gate.shape[0]
    experts = senders * local_experts
    route_count = routes.shape[1]
    capacity = max(2, 2 * rows_dev * route_count // experts)
    local_routed = None
    whole_gate, whole_up, whole_down = (
        lax.all_gather(expert_gate, "tp", axis=2, tiled=True),
        lax.all_gather(expert_up, "tp", axis=2, tiled=True),
        lax.all_gather(expert_down, "tp", axis=1, tiled=True),
    )
    own_routes = lax.dynamic_slice_in_dim(routes, column * rows_dev, rows_dev, 0)
    buffer, targets = build_buffer(normed, own_routes, experts, capacity)
    arrived = lax.all_to_all(buffer, "sp", split_axis=0, concat_axis=0, tiled=True)
    local_routed = whole_experts(
        arrived, whole_gate, whole_up, whole_down, senders, capacity, columns
    )
    shared_rows = lax.all_gather(normed[None], "tp", axis=0, tiled=True)
    shared_in = shared_rows
    shared_in = shared_in.reshape(1 * lax.axis_size("tp") * rows_dev, shared_in.shape[-1])
    shared_hidden = (
        jax.nn.silu(jnp.dot(shared_in, shared_gate, preferred_element_type=jnp.float32))
        * jnp.dot(shared_in, shared_up, preferred_element_type=jnp.float32)
    ).astype(jnp.bfloat16)
    shared_out = jnp.dot(shared_hidden, shared_down, preferred_element_type=jnp.float32)
    pieces = shared_out.reshape(1 * lax.axis_size("tp"), rows_dev, shared_out.shape[-1])
    terms_out = pieces.astype(jnp.bfloat16)
    summed = (
        lax.psum_scatter(
            lax.optimization_barrier(terms_out).astype(jnp.float32).astype(jnp.bfloat16),
            "tp",
            scatter_dimension=0,
            tiled=True,
        )
        .astype(jnp.float32)[0]
        .astype(jnp.bfloat16)
    )
    returned = lax.all_to_all(local_routed, "sp", split_axis=0, concat_axis=0, tiled=True)
    picked = (
        returned[targets].reshape(rows_dev, route_count, returned.shape[-1]).astype(jnp.float32)
    )
    routed_sum = jnp.sum(route_weight[:, :, None] * picked, axis=1)
    return (stream_wide + summed.astype(jnp.float32) + routed_sum).astype(jnp.bfloat16)


MESH = pl.DeviceIdType.MESH


def peer_barrier(peers):
    barrier = pltpu.get_barrier_semaphore()
    for peer in peers:
        pl.semaphore_signal(barrier, inc=1, device_id=peer, device_id_type=MESH)
    pl.semaphore_wait(barrier, len(peers))


def remote(src, dst, send_sem, recv_sem, peer):
    return pltpu.make_async_remote_copy(
        src_ref=src,
        dst_ref=dst,
        send_sem=send_sem,
        recv_sem=recv_sem,
        device_id=peer,
        device_id_type=MESH,
    )


def grid_place(sp):
    s = lax.axis_index("sp")
    t = lax.axis_index("tp")
    return s, t, s // 2, s % 2, sp // 2


def whole_kernel(sp, tp, *refs):
    lam_ref, query_ref, key_ref, value_ref, table_ref = refs[:5]
    residual_ref, head_gain_ref, norm_gain_ref = refs[5:8]
    out_weight, own_gate, own_up, own_sgate, own_sup, own_sdown, own_down = refs[8:15]
    out_ref = refs[15]
    kbuf, vbuf, qbuf, run_max, run_sum, run_acc, att_out, att_in, proj = refs[16:25]
    normed_ref, stream_ref, tab_in = refs[25:28]
    gate, up, down, sgate, sup, sdown = refs[28:34]
    rows, hid_own, hid_out, hid_in, parts, xin, zout, zin, sout, sin, total = refs[34:45]
    zs, zr, xs, xr, ys, yr, hs, hr, os_, or_, rs, rr, ss, sr = refs[45:59]
    kzs, kzr, kxs, kxr, hes, her, ns, nr, fs, fr, gs, gr, ts, tr, wsem = refs[59:]
    s, t, z, x, depth = grid_place(sp)
    count, width = normed_ref.shape
    quarter = own_gate.shape[1]
    tokens, lanes = key_ref.shape
    head_group = lam_ref.shape[0]
    y, c = t // 2, t % 2
    across = (z * 2 + (1 - x), t)
    mirror = (s, (1 - y) * 2 + c)
    partner = (s, y * 2 + 1 - c)
    opposite = (s, (1 - y) * 2 + 1 - c)
    line = [(lax.rem(z + k, depth) * 2 + x, t) for k in range(1, depth)]
    far_line = [(lax.rem(z + k, depth) * 2 + 1 - x, t) for k in range(1, depth)]
    first, second = pl.ds(0, quarter), pl.ds(quarter, quarter)
    started = []

    def send(source, target, send_sem, recv_sem, peer):
        copy = remote(source, target, send_sem, recv_sem, peer)
        copy.start()
        started.append(copy)
        return copy

    loads = [
        pltpu.make_async_copy(source, place, wsem.at[n])
        for n, (source, place) in enumerate(
            (
                (own_gate, gate.at[:, first]),
                (own_up, up.at[:, first]),
                (own_sgate, sgate.at[:, first]),
                (own_sup, sup.at[:, first]),
                (own_sdown, sdown.at[first]),
                (own_down, down.at[first]),
                (out_weight, proj),
            )
        )
    ]
    peer_barrier(line + far_line + [across, mirror, partner, opposite])
    keys_z, keys_x = {}, {}

    def send_keys_x(j):
        sources = (key_ref, value_ref) if j == 0 else (kbuf.at[j, 0], vbuf.at[j, 0])
        keys_x[j] = [
            send(source, buf.at[j, 1], kxs.at[i, j], kxr.at[i, j], across)
            for i, (source, buf) in enumerate(zip(sources, (kbuf, vbuf)))
        ]

    slabs = [1, 3, 2] if depth == 4 else list(range(1, depth))
    send_keys_x(0)
    for j in slabs:
        k = depth - j
        keys_z[j] = [
            send(source, buf.at[j, 0], kzs.at[i, k - 1], kzr.at[i, k - 1], line[k - 1])
            for i, (source, buf) in enumerate(((key_ref, kbuf), (value_ref, vbuf)))
        ]
    for n in (6, 0, 1, 2, 3, 4, 5):
        loads[n].start()
    pieces = fs.shape[0]
    piece = quarter // pieces
    far_down = []

    def send_far(n):
        far_down.append(
            send(
                own_down.at[pl.ds(n * piece, piece)],
                down.at[pl.ds(2 * quarter + n * piece, piece)],
                fs.at[n],
                fr.at[n],
                mirror,
            )
        )

    for n in range(pieces - 1):
        send_far(n)
    near = [
        send(source, place, ns.at[n], nr.at[n], partner)
        for n, (source, place) in enumerate(
            (
                (own_gate, gate.at[:, second]),
                (own_up, up.at[:, second]),
                (own_sgate, sgate.at[:, second]),
                (own_sup, sup.at[:, second]),
                (own_sdown, sdown.at[second]),
                (own_down, down.at[second]),
            )
        )
    ]
    tab_in[s] = table_ref[...]
    tables = [
        send(table_ref, tab_in.at[s], ts.at[n], tr.at[n], peer)
        for n, peer in enumerate(line + far_line + [across])
    ]

    kbuf[0, 0] = key_ref[...]
    vbuf[0, 0] = value_ref[...]
    lane = lax.broadcasted_iota(jnp.int32, (tokens, lanes), 1)
    for a in range(head_group):
        head_query = query_ref[:, a * lanes : (a + 1) * lanes]
        for i in range(2):
            mine = (lane >= i * (lanes // 2)) & (lane < (i + 1) * (lanes // 2))
            qbuf[2 * a + i] = jnp.where(mine, head_query, jnp.zeros_like(head_query))
    scale = (lanes // 2) ** (-0.5)

    def attend(j):
        for copy in keys_x[j]:
            copy.wait_recv()
        keys = kbuf[j].reshape(2 * tokens, lanes)
        values = vbuf[j].reshape(2 * tokens, vbuf.shape[3])
        for m in range(2 * head_group):
            scores = scale * lax.dot_general(
                qbuf[m], keys, (((1,), (1,)), ((), ())), preferred_element_type=jnp.float32
            )
            top = jnp.max(scores, axis=1, keepdims=True)
            if j != 0:
                old = run_max[m]
                top = jnp.maximum(old, top)
                shrink = jnp.exp(old - top)
            weights = jnp.exp(scores - top)
            row_sum = jnp.sum(weights, axis=1, keepdims=True)
            update = jnp.dot(
                weights.astype(jnp.bfloat16), values, preferred_element_type=jnp.float32
            )
            if j != 0:
                row_sum = row_sum + run_sum[m] * shrink
                update = update + run_acc[m] * shrink
            run_max[m] = top
            run_sum[m] = row_sum
            run_acc[m] = update

    def relay_keys(j):
        for copy in keys_z[j]:
            copy.wait_recv()
        send_keys_x(j)

    relay_keys(slabs[0])
    attend(0)
    relay_keys(slabs[1])
    attend(slabs[0])
    relay_keys(slabs[2])
    attend(slabs[1])
    attend(slabs[2])
    for a in range(head_group):
        value = run_acc[2 * a] / run_sum[2 * a] - lam_ref[a] * (
            run_acc[2 * a + 1] / run_sum[2 * a + 1]
        )
        rms = lax.rsqrt(jnp.mean(value * value, axis=1, keepdims=True) + norm_eps)
        att_out[a] = (value * rms * head_gain_ref[...]).astype(jnp.bfloat16)
    heads = [
        send(
            att_out.at[:, pl.ds(pl.multiple_of(peer[1] * count, 16), count)],
            att_in.at[pl.ds(head_group * t, head_group)],
            hes.at[n],
            her.at[n],
            peer,
        )
        for n, peer in enumerate((mirror, opposite, partner))
    ]
    send_far(pieces - 1)
    att_in[pl.ds(head_group * t, head_group)] = att_out[
        :, pl.ds(pl.multiple_of(t * count, 16), count)
    ]
    loads[6].wait()
    for copy in heads:
        copy.wait_recv()
    attended = jnp.concatenate([att_in[h] for h in range(tp * head_group)], axis=1)
    stream = (
        residual_ref[...].astype(jnp.float32)
        + jnp.dot(attended, proj[...], preferred_element_type=jnp.float32)
    ).astype(jnp.bfloat16)
    stream_ref[...] = stream
    wide = stream.astype(jnp.float32)
    inverse = lax.rsqrt(jnp.mean(wide * wide, axis=1, keepdims=True) + norm_eps)
    normed_ref[...] = (wide * inverse * norm_gain_ref[...]).astype(jnp.bfloat16)

    z_rows = {}
    x_rows, y_rows, diagonal, hids, x_outs, z_outs = {}, {}, {}, {}, {}, {}

    def own_rows(j):
        return normed_ref if j == 0 else rows.at[0, j, 0]

    def hidden_of(block, gate_buf, up_buf):
        gate_value = jnp.dot(block, gate_buf[...], preferred_element_type=jnp.float32)
        up_value = jnp.dot(block, up_buf[...], preferred_element_type=jnp.float32)
        return (jax.nn.silu(gate_value) * up_value).astype(jnp.bfloat16)

    waited = set()

    def arrived(copies, j):
        if (id(copies), j) not in waited:
            waited.add((id(copies), j))
            copies[j].wait_recv()

    def loaded(first_load, last_load):
        for n in range(first_load, last_load):
            if ("load", n) not in waited:
                waited.add(("load", n))
                loads[n].wait()
                near[n].wait_recv()

    def RX(j):
        if j != 0:
            arrived(z_rows, j)
        x_rows[j] = send(own_rows(j), rows.at[0, j, 1], xs.at[j], xr.at[j], across)

    def RY(j):
        if j != 0:
            arrived(z_rows, j)
        y_rows[j] = send(own_rows(j), rows.at[1, j, 0], ys.at[j], yr.at[j], mirror)

    def RD(j):
        sems = ys.at[depth + j], yr.at[depth + j]
        if j in by_x:
            arrived(y_rows, j)
            diagonal[j] = send(rows.at[1, j, 0], rows.at[1, j, 1], *sems, across)
        else:
            arrived(x_rows, j)
            diagonal[j] = send(rows.at[0, j, 1], rows.at[1, j, 1], *sems, mirror)

    def HO(j):
        arrived(x_rows, j)
        loaded(0, 2)
        hid_own[j] = hidden_of(rows[0, j].reshape(2 * count, width), gate, up)

    def HP(j):
        arrived(y_rows, j)
        arrived(diagonal, j)
        loaded(0, 2)
        hid_out[j] = hidden_of(rows[1, j].reshape(2 * count, width), gate, up)
        hids[j] = send(hid_out.at[j], hid_in.at[j], hs.at[j], hr.at[j], mirror)

    far_near = []

    def DR(j):
        for n, copy in enumerate(far_down):
            copy.wait_recv()
            far_near.append(
                send(
                    down.at[pl.ds(2 * quarter + n * piece, piece)],
                    down.at[pl.ds(3 * quarter + n * piece, piece)],
                    gs.at[n],
                    gr.at[n],
                    partner,
                )
            )

    def route_column(source):
        row = tab_in[source, pl.ds(s, 1)]
        shape = (count, row.shape[1])
        diagonal_mask = lax.broadcasted_iota(jnp.int32, shape, 0) == lax.broadcasted_iota(
            jnp.int32, shape, 1
        )
        spread = jnp.broadcast_to(row, shape)
        return jnp.sum(jnp.where(diagonal_mask, spread, 0.0), axis=1, keepdims=True)

    def FD(j):
        loaded(5, 6)
        for copies in (far_near, tables):
            if ("all", id(copies)) not in waited:
                waited.add(("all", id(copies)))
                for copy in copies:
                    copy.wait_recv()
        arrived(hids, j)
        half = hid_own.shape[2]
        value = jnp.dot(
            hid_own[j], down[pl.ds(0, half)], preferred_element_type=jnp.float32
        ) + jnp.dot(hid_in[j], down[pl.ds(half, half)], preferred_element_type=jnp.float32)
        base = lax.rem(z + j, depth) * 2
        parts[j, 1] = (value[count:] * route_column(base + 1 - x)).astype(jnp.bfloat16)
        x_outs[j] = send(parts.at[j, 1], xin.at[j], os_.at[j], or_.at[j], across)
        parts[j, 0] = (value[:count] * route_column(base + x)).astype(jnp.bfloat16)

    def FO(j):
        arrived(x_outs, j)
        zout[j - 1] = (parts[j, 0].astype(jnp.float32) + xin[j].astype(jnp.float32)).astype(
            jnp.bfloat16
        )
        z_outs[j] = send(
            zout.at[j - 1], zin.at[j - 1], rs.at[j - 1], rr.at[j - 1], line[j - 1]
        )

    shared_copy = []

    def SH(j):
        arrived(y_rows, 0)
        loaded(2, 5)
        pair = jnp.concatenate([normed_ref[...], rows[1, 0, 0]], axis=0)
        shared = jnp.dot(
            hidden_of(pair, sgate, sup), sdown[...], preferred_element_type=jnp.float32
        )
        sout[...] = shared[count:].astype(jnp.bfloat16)
        total[...] = stream_ref[...].astype(jnp.float32) + shared[:count]

    def SS(j):
        shared_copy.append(send(sout, sin, ss, sr, mirror))

    actions = {f.__name__: f for f in (RX, RY, RD, HO, HP, FD, FO, SH, SS, DR)}
    by_x, steps = moe_plan()
    rows[0, 0, 0] = normed_ref[...]
    for j in slabs:
        k = depth - j
        z_rows[j] = send(
            normed_ref, rows.at[0, j, 0], zs.at[k - 1], zr.at[k - 1], line[k - 1]
        )
    for step in steps:
        actions[step[:2]](int(step[2:] or 0))
    shared_copy[0].wait_recv()
    arrived(x_outs, 0)
    value = total[...] + sin[...].astype(jnp.float32)
    value = value + parts[0, 0].astype(jnp.float32) + xin[0].astype(jnp.float32)
    for j in range(1, depth):
        arrived(z_outs, j)
        value = value + zin[j - 1].astype(jnp.float32)
    out_ref[...] = value.astype(out_ref.dtype)
    for copy in started:
        copy.wait_send()


def moe_plan():
    return (0, 3), [
        step
        for group in (
            "RY0 RX0 RY1 RX1",
            "RY3 RX3 HO1 RD1",
            "RX2 RY2 RD3 HP1",
            "RD0 RD2 HO3 DR",
            "HP3",
            "FD1 HP2 FD3 FO1",
            "HP0 HO2 FD2 FO3",
            "HO0 FD0 FO2 SH",
            "SS",
        )
        for step in group.split()
    ]


def run_whole(scalars, small, large, tp, sp, collective_id):
    _, key, value, table, residual = small[:5]
    count, width = residual.shape
    tokens, lanes = key.shape
    head_group = scalars.shape[0]
    depth = sp // 2
    quarter = large[1].shape[1]
    half = 2 * quarter
    bf16, f32 = jnp.bfloat16, jnp.float32
    vmem = pl.BlockSpec(memory_space=pltpu.VMEM)
    pieces = 4

    def dma(*shape):
        return [pltpu.SemaphoreType.DMA(shape)] * 2

    maps = 2 * head_group
    scratch = [
        ((depth, 2, tokens, lanes), bf16),
        ((depth, 2, tokens, value.shape[1]), bf16),
        ((maps, tokens, lanes), bf16),
        ((maps, tokens, 1), f32),
        ((maps, tokens, 1), f32),
        ((maps, tokens, value.shape[1]), f32),
        ((head_group, tokens, value.shape[1]), bf16),
        ((tp * head_group, count, value.shape[1]), bf16),
        (large[0].shape, bf16),
        ((count, width), bf16),
        ((count, width), bf16),
        ((sp,) + table.shape, f32),
        ((width, half), bf16),
        ((width, half), bf16),
        ((2 * half, width), bf16),
        ((width, half), bf16),
        ((width, half), bf16),
        ((half, width), bf16),
        ((2, depth, 2, count, width), bf16),
        ((depth, 2 * count, half), bf16),
        ((depth, 2 * count, half), bf16),
        ((depth, 2 * count, half), bf16),
        ((depth, 2, count, width), bf16),
        ((depth, count, width), bf16),
        ((depth - 1, count, width), bf16),
        ((depth - 1, count, width), bf16),
        ((count, width), bf16),
        ((count, width), bf16),
        ((count, width), f32),
    ]
    return pl.pallas_call(
        partial(whole_kernel, sp, tp),
        out_shape=jax.ShapeDtypeStruct((count, width), bf16),
        in_specs=[pl.BlockSpec(memory_space=pltpu.SMEM)]
        + [vmem] * len(small)
        + [pl.BlockSpec(memory_space=pl.ANY)] * len(large),
        out_specs=vmem,
        scratch_shapes=[pltpu.VMEM(shape, dtype) for shape, dtype in scratch]
        + dma(depth - 1)
        + dma(depth)
        + dma(2 * depth)
        + dma(depth)
        + dma(depth)
        + dma(depth - 1)
        + [pltpu.SemaphoreType.DMA] * 2
        + dma(2, depth - 1)
        + dma(2, depth)
        + dma(tp - 1)
        + dma(6)
        + dma(pieces)
        + dma(pieces)
        + dma(sp - 1)
        + [pltpu.SemaphoreType.DMA((len(large),))],
        compiler_params=pltpu.CompilerParams(
            collective_id=collective_id,
            has_side_effects=True,
            vmem_limit_bytes=58 * 1024 * 1024,
        ),
        cost_estimate=pl.CostEstimate(
            flops=12 * depth * count * width * half * 3,
            bytes_accessed=30_000_000,
            transcendentals=0,
        ),
    )(scalars, *small, *large)


def dense_body(
    query_maps,
    key_maps,
    value_rows,
    mix_lambda,
    head_gain,
    out_weight,
    residual,
    norm_gain,
    routes,
    route_weight,
    expert_gate,
    expert_up,
    expert_down,
    shared_gate,
    shared_up,
    shared_down,
):
    sp = lax.axis_size("sp")
    tp = lax.axis_size("tp")
    t = lax.axis_index("tp")
    head_width = head_gain.shape[0]
    rows_dev = residual.shape[0]
    width = residual.shape[1]
    own_routes = lax.dynamic_slice_in_dim(routes, t * rows_dev, rows_dev, 0)
    named = own_routes[None, :, :] == jnp.arange(sp, dtype=jnp.int32)[:, None, None]
    table = jnp.sum(jnp.where(named, route_weight[None], 0.0), axis=2)
    lanes = -(-rows_dev // 128) * 128
    table = jnp.pad(table, ((0, 0), (0, lanes - rows_dev)))
    return run_whole(
        mix_lambda,
        (
            query_maps,
            key_maps,
            value_rows,
            table,
            residual,
            head_gain.reshape(1, head_width),
            norm_gain.reshape(1, width),
        ),
        (
            out_weight,
            expert_gate[0],
            expert_up[0],
            shared_gate,
            shared_up,
            shared_down,
            expert_down[0],
        ),
        tp,
        sp,
        1,
    )


def solution(mesh):
    in_specs = (
        P("sp", "tp"),
        P("sp", "tp"),
        P("sp", "tp"),
        P("tp"),
        P(),
        P(),
        P(("sp", "tp"), None),
        P(),
        P("sp", None),
        P(("sp", "tp"), None),
        P("sp", None, "tp"),
        P("sp", None, "tp"),
        P("sp", "tp", None),
        P(None, "tp"),
        P(None, "tp"),
        P("tp", None),
    )
    out_specs = P(("sp", "tp"), None)
    sp, tp = mesh.shape["sp"], mesh.shape["tp"]

    def chosen(*args):
        route_count = args[8].shape[1]
        experts = sp * args[10].shape[0]
        rows_dev = args[6].shape[0]
        whole_blocks = 2 * rows_dev * route_count >= experts * rows_dev
        kv_local = args[2].shape[1] // args[4].shape[0]
        dense = whole_blocks and args[10].shape[0] == 1 and sp == 8 and tp == 4 and kv_local == 1
        if not dense:
            return body(*args)
        return dense_body(*args)

    return jax.shard_map(
        chosen, mesh=mesh, in_specs=in_specs, out_specs=out_specs, check_vma=False
    )
```

time: 106 us -> 92.8 us (0.88)
  matrix products: 10.3 us -> 0 us
  Pallas kernels: 82.8 us -> 88.9 us
  starting transfers between devices: 4.66 us -> 0 us
  other arithmetic: 3.86 us -> 0.69 us
  local copies, waits for them, and re-layouts: 4.07 us -> 2.97 us
    dot_general x7 -> x0, matrix products: 10.3 us -> none  [the longest x3 5.41 us: attention_block(): jnp.einsum('agcqr,rae->agcqe', weights.astype(jnp.bfloat16), value_heads,...]
    pallas_call x3 -> x1, Pallas kernels: 82.8 us -> 88.9 us  [run_whole(): pl.pallas_call(partial(whole_kernel, sp, tp), out_shape=jax.ShapeDtypeStr...]
    ppermute x8 -> x0, starting transfers between devices: 4.66 us -> none  [swapped(): return lax.ppermute(array, 'tp', [(i, i ^ step) for i in range(tp)])]
    another operation x3 -> x0, other arithmetic: 1.35 us -> none
    div x1 -> x0, other arithmetic: 1.25 us -> none  [dense_body(): normalized = accumulated / run_sum[..., None]]
    unnamed x26 -> x3, local copies, waits for them, and re-layouts: 3.34 us -> 2.3 us
  transfers between devices with their start and end apart: 8 -> 0, of which waited for: 0 -> 0; matrix products, arithmetic and copies ran while one was open for 15% -> 0% of each run, Pallas kernels for 22% -> 0%
where the time goes in v2:
time: 92.8 us; the launch traced here: 92.6 us
  Pallas kernels  88.9 us (96%)
  local copies, waits for them, and re-layouts  2.97 us (3%)
    pallas_call x1, Pallas kernels, run_whole(): pl.pallas_call(partial(whole_kernel, sp, tp), out_shape=jax.ShapeDtypeStr...  88.9 us
    unnamed x3, local copies, waits for them, and re-layouts  2.3 us

profile of v2, /device:TPU:0, one launch (start us, length us, event | category | flops | bytes accessed | tf_op | source)
XLA Modules:
  0.0 92.6 jit_solution(1470009016499583987)
XLA Ops:
  0.0 0.0 copy-start
  0.0 0.7 copy-done
  0.7 0.1 constant_dynamic-slice_fusion
  0.8 0.7 select_reduce_fusion
  1.5 0.6 pad.4.refs_4_
  2.1 88.9 %shard_map.154 = bf16[48,2048]{1,0:T(8,128)(2,1)} custom-call(f32[2]{0:T(128)} %refs_0_.1, bf16[192,256]{1,0:T(8,128)(2,1)} %refs_1_.1, bf16[192,128]{1,0:T(8,128)(2,1)} %refs_2_.1, bf16[192,128]{1,0:T(8,128)(2,1)} %refs_3_.1, f32[8,128]{1,0:T(8,128)} %pad.4.refs_4_, bf16[48,2048]{1,0:T(8,128)(2,1)} %refs_5_.1, f32[1,128]{1,0:T(1,128)} %bitcast.9, ...), custom_call_target="tpu_custom_call" | custom-call | flops 7247757312 | bytes 30000000 | tf_op jit(solution)/shard_map/pallas_call | solution.py:627
  91.0 1.6 %copy.20 = bf16[48,2048]{1,0:T(8,128)(2,1)} copy(bf16[48,2048]{1,0:T(8,128)(2,1)} %shard_map.154) | data formatting | bytes 393216
Async XLA Ops:
  0.0 0.7 copy-start

commit v3 on v2

--- a/solution.py
+++ b/solution.py
@@ -209,13 +209,6 @@
 MESH = pl.DeviceIdType.MESH
 
 
-def peer_barrier(peers):
-    barrier = pltpu.get_barrier_semaphore()
-    for peer in peers:
-        pl.semaphore_signal(barrier, inc=1, device_id=peer, device_id_type=MESH)
-    pl.semaphore_wait(barrier, len(peers))
-
-
 def remote(src, dst, send_sem, recv_sem, peer):
     return pltpu.make_async_remote_copy(
         src_ref=src,
@@ -234,20 +227,21 @@
 
 
 def whole_kernel(sp, tp, *refs):
-    lam_ref, query_ref, key_ref, value_ref, table_ref = refs[:5]
-    residual_ref, head_gain_ref, norm_gain_ref = refs[5:8]
-    out_weight, own_gate, own_up, own_sgate, own_sup, own_sdown, own_down = refs[8:15]
-    out_ref = refs[15]
-    kbuf, vbuf, qbuf, run_max, run_sum, run_acc, att_out, att_in, proj = refs[16:25]
-    normed_ref, stream_ref, tab_in = refs[25:28]
-    gate, up, down, sgate, sup, sdown = refs[28:34]
-    rows, hid_own, hid_out, hid_in, parts, xin, zout, zin, sout, sin, total = refs[34:45]
-    zs, zr, xs, xr, ys, yr, hs, hr, os_, or_, rs, rr, ss, sr = refs[45:59]
-    kzs, kzr, kxs, kxr, hes, her, ns, nr, fs, fr, gs, gr, ts, tr, wsem = refs[59:]
+    inputs, small = refs[:9], refs[17:25]
+    out_weight, own_gate, own_up, own_sgate, own_sup, own_sdown, own_down = refs[9:16]
+    out_ref = refs[16]
+    query_ref, lam_ref, routes_ref, route_weight_ref = small[:4]
+    residual_ref, head_gain_ref, norm_gain_ref, table_ref = small[4:]
+    kbuf, vbuf, qbuf, run_max, run_sum, run_acc, att_out, att_in, proj = refs[25:34]
+    normed_ref, stream_ref, tab_in = refs[34:37]
+    gate, up, down, sgate, sup, sdown = refs[37:43]
+    rows, hid_own, hid_out, hid_in, parts, xin, zout, zin, sout, sin, total = refs[43:54]
+    zs, zr, xs, xr, ys, yr, hs, hr, os_, or_, rs, rr, ss, sr = refs[54:68]
+    kzs, kzr, kxs, kxr, hes, her, ns, nr, fs, fr, gs, gr, ts, tr, wsem, isem = refs[68:]
     s, t, z, x, depth = grid_place(sp)
     count, width = normed_ref.shape
     quarter = own_gate.shape[1]
-    tokens, lanes = key_ref.shape
+    tokens, lanes = kbuf.shape[2:]
     head_group = lam_ref.shape[0]
     y, c = t // 2, t % 2
     across = (z * 2 + (1 - x), t)
@@ -279,14 +273,40 @@
             )
         )
     ]
-    peer_barrier(line + far_line + [across, mirror, partner, opposite])
+    peers = line + far_line + [across, mirror, partner, opposite]
+    barrier = pltpu.get_barrier_semaphore()
+    for peer in peers:
+        pl.semaphore_signal(barrier, inc=1, device_id=peer, device_id_type=MESH)
+    fetches = [
+        pltpu.make_async_copy(source, place, isem.at[n])
+        for n, (source, place) in enumerate(
+            zip(
+                inputs,
+                (
+                    kbuf.at[0, 0],
+                    vbuf.at[0, 0],
+                    query_ref,
+                    lam_ref,
+                    routes_ref,
+                    route_weight_ref,
+                    residual_ref,
+                    head_gain_ref,
+                    norm_gain_ref,
+                ),
+            )
+        )
+    ]
+    for fetch in fetches:
+        fetch.start()
+    fetches[0].wait()
+    fetches[1].wait()
+    pl.semaphore_wait(barrier, len(peers))
     keys_z, keys_x = {}, {}
 
     def send_keys_x(j):
-        sources = (key_ref, value_ref) if j == 0 else (kbuf.at[j, 0], vbuf.at[j, 0])
         keys_x[j] = [
-            send(source, buf.at[j, 1], kxs.at[i, j], kxr.at[i, j], across)
-            for i, (source, buf) in enumerate(zip(sources, (kbuf, vbuf)))
+            send(buf.at[j, 0], buf.at[j, 1], kxs.at[i, j], kxr.at[i, j], across)
+            for i, buf in enumerate((kbuf, vbuf))
         ]
 
     slabs = [1, 3, 2] if depth == 4 else list(range(1, depth))
@@ -294,12 +314,13 @@
     for j in slabs:
         k = depth - j
         keys_z[j] = [
-            send(source, buf.at[j, 0], kzs.at[i, k - 1], kzr.at[i, k - 1], line[k - 1])
-            for i, (source, buf) in enumerate(((key_ref, kbuf), (value_ref, vbuf)))
+            send(buf.at[0, 0], buf.at[j, 0], kzs.at[i, k - 1], kzr.at[i, k - 1], line[k - 1])
+            for i, buf in enumerate((kbuf, vbuf))
         ]
     for n in (6, 0, 1, 2, 3, 4, 5):
         loads[n].start()
     pieces = fs.shape[0]
+    early = pieces - 2
     piece = quarter // pieces
     far_down = []
 
@@ -314,8 +335,8 @@
             )
         )
 
-    for n in range(pieces - 1):
-        send_far(n)
+    send_far(0)
+    send_far(1)
     near = [
         send(source, place, ns.at[n], nr.at[n], partner)
         for n, (source, place) in enumerate(
@@ -329,14 +350,8 @@
             )
         )
     ]
-    tab_in[s] = table_ref[...]
-    tables = [
-        send(table_ref, tab_in.at[s], ts.at[n], tr.at[n], peer)
-        for n, peer in enumerate(line + far_line + [across])
-    ]
-
-    kbuf[0, 0] = key_ref[...]
-    vbuf[0, 0] = value_ref[...]
+    for fetch in fetches[2:]:
+        fetch.wait()
     lane = lax.broadcasted_iota(jnp.int32, (tokens, lanes), 1)
     for a in range(head_group):
         head_query = query_ref[:, a * lanes : (a + 1) * lanes]
@@ -345,11 +360,12 @@
             qbuf[2 * a + i] = jnp.where(mine, head_query, jnp.zeros_like(head_query))
     scale = (lanes // 2) ** (-0.5)
 
-    def attend(j):
-        for copy in keys_x[j]:
-            copy.wait_recv()
-        keys = kbuf[j].reshape(2 * tokens, lanes)
-        values = vbuf[j].reshape(2 * tokens, vbuf.shape[3])
+    def attend(j, low=0, high=2):
+        if high == 2:
+            for copy in keys_x[j]:
+                copy.wait_recv()
+        keys = kbuf[j, low:high].reshape((high - low) * tokens, lanes)
+        values = vbuf[j, low:high].reshape((high - low) * tokens, vbuf.shape[3])
         for m in range(2 * head_group):
             scores = scale * lax.dot_general(
                 qbuf[m], keys, (((1,), (1,)), ((), ())), preferred_element_type=jnp.float32
@@ -376,13 +392,37 @@
             copy.wait_recv()
         send_keys_x(j)
 
+    def build_table():
+        chosen = routes_ref[:, :count]
+        for n in range(1, tp):
+            chosen = jnp.where(t == n, routes_ref[:, n * count : (n + 1) * count], chosen)
+        names = [
+            jnp.sum(
+                jnp.where(chosen == expert, route_weight_ref[...], 0.0), axis=0, keepdims=True
+            )
+            for expert in range(sp)
+        ]
+        table = jnp.concatenate(names, axis=0)
+        spare = jnp.zeros((sp, table_ref.shape[1] - count), jnp.float32)
+        table_ref[...] = jnp.concatenate([table, spare], axis=1)
+        tab_in[s] = table_ref[...]
+        return [
+            send(table_ref, tab_in.at[s], ts.at[n], tr.at[n], peer)
+            for n, peer in enumerate(line + far_line + [across])
+        ]
+
     relay_keys(slabs[0])
+    send_far(2)
     attend(0)
     relay_keys(slabs[1])
     attend(slabs[0])
+    send_far(3)
     relay_keys(slabs[2])
+    attend(slabs[2], 0, 1)
+    tables = build_table()
     attend(slabs[1])
-    attend(slabs[2])
+    send_far(4)
+    attend(slabs[2], 1, 2)
     for a in range(head_group):
         value = run_acc[2 * a] / run_sum[2 * a] - lam_ref[a] * (
             run_acc[2 * a + 1] / run_sum[2 * a + 1]
@@ -399,7 +439,8 @@
         )
         for n, peer in enumerate((mirror, opposite, partner))
     ]
-    send_far(pieces - 1)
+    for n in range(5, early):
+        send_far(n)
     att_in[pl.ds(head_group * t, head_group)] = att_out[
         :, pl.ds(pl.multiple_of(t * count, 16), count)
     ]
@@ -418,21 +459,25 @@
 
     z_rows = {}
     x_rows, y_rows, diagonal, hids, x_outs, z_outs = {}, {}, {}, {}, {}, {}
-
-    def own_rows(j):
-        return normed_ref if j == 0 else rows.at[0, j, 0]
+    half_width = width // 2
+    waited = set()
+
+    def part(ref, h):
+        return ref.at[:, pl.ds(h * half_width, half_width)]
+
+    def own_rows(j, h):
+        return part(normed_ref if j == 0 else rows.at[0, j, 0], h)
 
     def hidden_of(block, gate_buf, up_buf):
         gate_value = jnp.dot(block, gate_buf[...], preferred_element_type=jnp.float32)
         up_value = jnp.dot(block, up_buf[...], preferred_element_type=jnp.float32)
         return (jax.nn.silu(gate_value) * up_value).astype(jnp.bfloat16)
 
-    waited = set()
-
-    def arrived(copies, j):
-        if (id(copies), j) not in waited:
-            waited.add((id(copies), j))
-            copies[j].wait_recv()
+    def arrived(copies, *keys):
+        for key in keys:
+            if (id(copies), key) not in waited:
+                waited.add((id(copies), key))
+                copies[key].wait_recv()
 
     def loaded(first_load, last_load):
         for n in range(first_load, last_load):
@@ -441,40 +486,57 @@
                 loads[n].wait()
                 near[n].wait_recv()
 
-    def RX(j):
+    def RX(j, h):
         if j != 0:
-            arrived(z_rows, j)
-        x_rows[j] = send(own_rows(j), rows.at[0, j, 1], xs.at[j], xr.at[j], across)
-
-    def RY(j):
+            arrived(z_rows, (j, h))
+        x_rows[j, h] = send(
+            own_rows(j, h), part(rows.at[0, j, 1], h), xs.at[j, h], xr.at[j, h], across
+        )
+
+    def RY(j, h):
+        sems = ys.at[j, h], yr.at[j, h]
+        if j in by_z:
+            arrived(y_rows, (0, h))
+            y_rows[j, h] = send(
+                part(rows.at[1, 0, 0], h), part(rows.at[1, j, 0], h), *sems, line[depth - j - 1]
+            )
+            return
         if j != 0:
-            arrived(z_rows, j)
-        y_rows[j] = send(own_rows(j), rows.at[1, j, 0], ys.at[j], yr.at[j], mirror)
-
-    def RD(j):
-        sems = ys.at[depth + j], yr.at[depth + j]
+            arrived(z_rows, (j, h))
+        y_rows[j, h] = send(own_rows(j, h), part(rows.at[1, j, 0], h), *sems, mirror)
+
+    def RD(j, h):
+        sems = ys.at[depth + j, h], yr.at[depth + j, h]
+        target = part(rows.at[1, j, 1], h)
         if j in by_x:
-            arrived(y_rows, j)
-            diagonal[j] = send(rows.at[1, j, 0], rows.at[1, j, 1], *sems, across)
+            arrived(y_rows, (j, h))
+            diagonal[j, h] = send(part(rows.at[1, j, 0], h), target, *sems, across)
         else:
-            arrived(x_rows, j)
-            diagonal[j] = send(rows.at[0, j, 1], rows.at[1, j, 1], *sems, mirror)
-
-    def HO(j):
-        arrived(x_rows, j)
+            arrived(x_rows, (j, h))
+            diagonal[j, h] = send(part(rows.at[0, j, 1], h), target, *sems, mirror)
+
+    def HO(j, h):
+        if j != 0:
+            arrived(z_rows, (j, 0), (j, 1))
+        arrived(x_rows, (j, 0), (j, 1))
         loaded(0, 2)
         hid_own[j] = hidden_of(rows[0, j].reshape(2 * count, width), gate, up)
 
-    def HP(j):
-        arrived(y_rows, j)
-        arrived(diagonal, j)
+    def HP(j, h):
+        arrived(y_rows, (j, 0), (j, 1))
+        arrived(diagonal, (j, 0), (j, 1))
         loaded(0, 2)
         hid_out[j] = hidden_of(rows[1, j].reshape(2 * count, width), gate, up)
         hids[j] = send(hid_out.at[j], hid_in.at[j], hs.at[j], hr.at[j], mirror)
 
     far_near = []
 
-    def DR(j):
+    def FR(j, h):
+        for n in range(j, pieces):
+            if n == j or h:
+                send_far(n)
+
+    def DR(j, h):
         for n, copy in enumerate(far_down):
             copy.wait_recv()
             far_near.append(
@@ -496,7 +558,7 @@
         spread = jnp.broadcast_to(row, shape)
         return jnp.sum(jnp.where(diagonal_mask, spread, 0.0), axis=1, keepdims=True)
 
-    def FD(j):
+    def FD(j, h):
         loaded(5, 6)
         for copies in (far_near, tables):
             if ("all", id(copies)) not in waited:
@@ -505,27 +567,39 @@
                     copy.wait_recv()
         arrived(hids, j)
         half = hid_own.shape[2]
+        columns = pl.ds(h * half_width, half_width)
         value = jnp.dot(
-            hid_own[j], down[pl.ds(0, half)], preferred_element_type=jnp.float32
-        ) + jnp.dot(hid_in[j], down[pl.ds(half, half)], preferred_element_type=jnp.float32)
+            hid_own[j], down[pl.ds(0, half), columns], preferred_element_type=jnp.float32
+        ) + jnp.dot(
+            hid_in[j], down[pl.ds(half, half), columns], preferred_element_type=jnp.float32
+        )
         base = lax.rem(z + j, depth) * 2
-        parts[j, 1] = (value[count:] * route_column(base + 1 - x)).astype(jnp.bfloat16)
-        x_outs[j] = send(parts.at[j, 1], xin.at[j], os_.at[j], or_.at[j], across)
-        parts[j, 0] = (value[:count] * route_column(base + x)).astype(jnp.bfloat16)
-
-    def FO(j):
-        arrived(x_outs, j)
-        zout[j - 1] = (parts[j, 0].astype(jnp.float32) + xin[j].astype(jnp.float32)).astype(
+        parts[j, 1, :, columns] = (value[count:] * route_column(base + 1 - x)).astype(
             jnp.bfloat16
         )
-        z_outs[j] = send(
-            zout.at[j - 1], zin.at[j - 1], rs.at[j - 1], rr.at[j - 1], line[j - 1]
+        x_outs[j, h] = send(
+            part(parts.at[j, 1], h), part(xin.at[j], h), os_.at[j, h], or_.at[j, h], across
+        )
+        parts[j, 0, :, columns] = (value[:count] * route_column(base + x)).astype(jnp.bfloat16)
+
+    def FO(j, h):
+        arrived(x_outs, (j, h))
+        columns = pl.ds(h * half_width, half_width)
+        zout[j - 1, :, columns] = (
+            parts[j, 0, :, columns].astype(jnp.float32) + xin[j, :, columns].astype(jnp.float32)
+        ).astype(jnp.bfloat16)
+        z_outs[j, h] = send(
+            part(zout.at[j - 1], h),
+            part(zin.at[j - 1], h),
+            rs.at[j - 1, h],
+            rr.at[j - 1, h],
+            line[j - 1],
         )
 
     shared_copy = []
 
-    def SH(j):
-        arrived(y_rows, 0)
+    def SH(j, h):
+        arrived(y_rows, (0, 0), (0, 1))
         loaded(2, 5)
         pair = jnp.concatenate([normed_ref[...], rows[1, 0, 0]], axis=0)
         shared = jnp.dot(
@@ -534,25 +608,31 @@
         sout[...] = shared[count:].astype(jnp.bfloat16)
         total[...] = stream_ref[...].astype(jnp.float32) + shared[:count]
 
-    def SS(j):
+    def SS(j, h):
         shared_copy.append(send(sout, sin, ss, sr, mirror))
 
-    actions = {f.__name__: f for f in (RX, RY, RD, HO, HP, FD, FO, SH, SS, DR)}
-    by_x, steps = moe_plan()
+    actions = {f.__name__: f for f in (RX, RY, RD, HO, HP, FD, FO, SH, SS, DR, FR)}
+    by_x, by_z, steps = moe_plan()
     rows[0, 0, 0] = normed_ref[...]
     for j in slabs:
         k = depth - j
-        z_rows[j] = send(
-            normed_ref, rows.at[0, j, 0], zs.at[k - 1], zr.at[k - 1], line[k - 1]
-        )
+        for h in range(2):
+            z_rows[j, h] = send(
+                part(normed_ref, h),
+                part(rows.at[0, j, 0], h),
+                zs.at[k - 1, h],
+                zr.at[k - 1, h],
+                line[k - 1],
+            )
     for step in steps:
-        actions[step[:2]](int(step[2:] or 0))
+        number = int(step[2:3] or 0)
+        actions[step[:2]](number, "ab".index(step[3:4] or "a"))
     shared_copy[0].wait_recv()
-    arrived(x_outs, 0)
+    arrived(x_outs, (0, 0), (0, 1))
     value = total[...] + sin[...].astype(jnp.float32)
     value = value + parts[0, 0].astype(jnp.float32) + xin[0].astype(jnp.float32)
     for j in range(1, depth):
-        arrived(z_outs, j)
+        arrived(z_outs, (j, 0), (j, 1))
         value = value + zin[j - 1].astype(jnp.float32)
     out_ref[...] = value.astype(out_ref.dtype)
     for copy in started:
@@ -560,34 +640,39 @@
 
 
 def moe_plan():
-    return (0, 3), [
+    return (1, 2), (3,), [
         step
         for group in (
-            "RY0 RX0 RY1 RX1",
-            "RY3 RX3 HO1 RD1",
-            "RX2 RY2 RD3 HP1",
-            "RD0 RD2 HO3 DR",
-            "HP3",
-            "FD1 HP2 FD3 FO1",
-            "HP0 HO2 FD2 FO3",
-            "HO0 FD0 FO2 SH",
-            "SS",
+            "RX0a RX0b FR6 FR7",
+            "RY1a RX1a RX1b RY1b",
+            "RY0b RY0a RX3a RX3b",
+            "RD1b RY2a DR RD1a",
+            "RY2b RD3a RY3b RX2a",
+            "SH RX2b HO0 RD2a",
+            "RY3a RD3b RD2b HP1",
+            "HO1 RD0a HP3 FD1a",
+            "FD1b RD0b HO3 HP2",
+            "FD3a SS FO1a HO2",
+            "FD3b FO1b FD2b FO3a",
+            "HP0 FD2a FO3b FO2b",
+            "FD0b FD0a FO2a",
         )
         for step in group.split()
     ]
 
 
-def run_whole(scalars, small, large, tp, sp, collective_id):
-    _, key, value, table, residual = small[:5]
+def run_whole(small, large, tp, sp, collective_id):
+    key, value, query, _, routes, route_weight, residual, head_gain, norm_gain = small
     count, width = residual.shape
     tokens, lanes = key.shape
-    head_group = scalars.shape[0]
+    head_group = small[3].shape[0]
     depth = sp // 2
     quarter = large[1].shape[1]
     half = 2 * quarter
     bf16, f32 = jnp.bfloat16, jnp.float32
     vmem = pl.BlockSpec(memory_space=pltpu.VMEM)
-    pieces = 4
+    pieces = 8
+    table = (sp, -(-count // 128) * 128)
 
     def dma(*shape):
         return [pltpu.SemaphoreType.DMA(shape)] * 2
@@ -605,7 +690,7 @@
         (large[0].shape, bf16),
         ((count, width), bf16),
         ((count, width), bf16),
-        ((sp,) + table.shape, f32),
+        ((sp,) + table, f32),
         ((width, half), bf16),
         ((width, half), bf16),
         ((2 * half, width), bf16),
@@ -627,17 +712,25 @@
     return pl.pallas_call(
         partial(whole_kernel, sp, tp),
         out_shape=jax.ShapeDtypeStruct((count, width), bf16),
-        in_specs=[pl.BlockSpec(memory_space=pltpu.SMEM)]
-        + [vmem] * len(small)
-        + [pl.BlockSpec(memory_space=pl.ANY)] * len(large),
+        in_specs=[pl.BlockSpec(memory_space=pltpu.HBM)] * (len(small) + len(large)),
         out_specs=vmem,
-        scratch_shapes=[pltpu.VMEM(shape, dtype) for shape, dtype in scratch]
-        + dma(depth - 1)
+        scratch_shapes=[
+            pltpu.VMEM(query.shape, bf16),
+            pltpu.SMEM(small[3].shape, f32),
+            pltpu.VMEM(routes.shape, jnp.int32),
+            pltpu.VMEM(route_weight.shape, f32),
+            pltpu.VMEM(residual.shape, bf16),
+            pltpu.VMEM(head_gain.shape, f32),
+            pltpu.VMEM(norm_gain.shape, f32),
+            pltpu.VMEM(table, f32),
+        ]
+        + [pltpu.VMEM(shape, dtype) for shape, dtype in scratch]
+        + dma(depth - 1, 2)
+        + dma(depth, 2)
+        + dma(2 * depth, 2)
         + dma(depth)
-        + dma(2 * depth)
-        + dma(depth)
-        + dma(depth)
-        + dma(depth - 1)
+        + dma(depth, 2)
+        + dma(depth - 1, 2)
         + [pltpu.SemaphoreType.DMA] * 2
         + dma(2, depth - 1)
         + dma(2, depth)
@@ -646,18 +739,18 @@
         + dma(pieces)
         + dma(pieces)
         + dma(sp - 1)
-        + [pltpu.SemaphoreType.DMA((len(large),))],
+        + [pltpu.SemaphoreType.DMA((len(large),)), pltpu.SemaphoreType.DMA((len(small),))],
         compiler_params=pltpu.CompilerParams(
             collective_id=collective_id,
             has_side_effects=True,
-            vmem_limit_bytes=58 * 1024 * 1024,
+            vmem_limit_bytes=56 * 1024 * 1024,
         ),
         cost_estimate=pl.CostEstimate(
             flops=12 * depth * count * width * half * 3,
             bytes_accessed=30_000_000,
             transcendentals=0,
         ),
-    )(scalars, *small, *large)
+    )(*small, *large)
 
 
 def dense_body(
@@ -680,25 +773,17 @@
 ):
     sp = lax.axis_size("sp")
     tp = lax.axis_size("tp")
-    t = lax.axis_index("tp")
-    head_width = head_gain.shape[0]
-    rows_dev = residual.shape[0]
-    width = residual.shape[1]
-    own_routes = lax.dynamic_slice_in_dim(routes, t * rows_dev, rows_dev, 0)
-    named = own_routes[None, :, :] == jnp.arange(sp, dtype=jnp.int32)[:, None, None]
-    table = jnp.sum(jnp.where(named, route_weight[None], 0.0), axis=2)
-    lanes = -(-rows_dev // 128) * 128
-    table = jnp.pad(table, ((0, 0), (0, lanes - rows_dev)))
     return run_whole(
-        mix_lambda,
         (
-            query_maps,
             key_maps,
             value_rows,
-            table,
+            query_maps,
+            mix_lambda,
+            routes.T,
+            route_weight.T,
             residual,
-            head_gain.reshape(1, head_width),
-            norm_gain.reshape(1, width),
+            head_gain.reshape(1, -1),
+            norm_gain.reshape(1, -1),
         ),
         (
             out_weight,

time: 92.8 us -> 84.9 us (0.915)
  Pallas kernels: 88.9 us -> 83.1 us
  local copies, waits for them, and re-layouts: 2.97 us -> 1.62 us
    pallas_call x1, Pallas kernels: 88.9 us -> 83.1 us  [run_whole(): pl.pallas_call(partial(whole_kernel, sp, tp), out_shape=jax.ShapeDtypeStr...]
    unnamed x3 -> x1, local copies, waits for them, and re-layouts: 2.3 us -> 1.62 us
where the time goes in v3:
time: 84.9 us; the launch traced here: 84.8 us
  Pallas kernels  83.1 us (98%)
  local copies, waits for them, and re-layouts  1.62 us (2%)
    pallas_call x1, Pallas kernels, run_whole(): pl.pallas_call(partial(whole_kernel, sp, tp), out_shape=jax.ShapeDtypeStr...  83.1 us

profile of v3, /device:TPU:0, one launch (start us, length us, event | category | flops | bytes accessed | tf_op | source)
XLA Modules:
  0.0 84.8 jit_solution(171800135693446395)
XLA Ops:
  0.0 83.1 %shard_map.154 = bf16[48,2048]{1,0:T(8,128)(2,1)} custom-call(bf16[192,128]{1,0:T(8,128)(2,1)} %refs_0_.1, bf16[192,128]{1,0:T(8,128)(2,1)} %refs_1_.1, bf16[192,256]{1,0:T(8,128)(2,1)} %refs_2_.1, f32[2]{0:T(128)} %refs_3_.1, s32[4,192]{1,0:T(4,128)} %bitcast.11, f32[4,48]{1,0:T(4,128)} %bitcast.12, bf16[48,2048]{1,0:T(8,128)(2,1)} %refs_6_.1, ...), custom_call_target="tpu_custom_call" | custom-call | flops 7247757312 | bytes 30000000 | tf_op jit(solution)/shard_map/pallas_call | solution.py:712
  83.2 1.6 %copy.18 = bf16[48,2048]{1,0:T(8,128)(2,1)} copy(bf16[48,2048]{1,0:T(8,128)(2,1)} %shard_map.154) | data formatting | bytes 393216

commit v4 on v3

--- a/solution.py
+++ b/solution.py
@@ -1,3 +1,4 @@
+import math
 from functools import partial
 
 import jax
@@ -232,12 +233,12 @@
     out_ref = refs[16]
     query_ref, lam_ref, routes_ref, route_weight_ref = small[:4]
     residual_ref, head_gain_ref, norm_gain_ref, table_ref = small[4:]
-    kbuf, vbuf, qbuf, run_max, run_sum, run_acc, att_out, att_in, proj = refs[25:34]
-    normed_ref, stream_ref, tab_in = refs[34:37]
-    gate, up, down, sgate, sup, sdown = refs[37:43]
-    rows, hid_own, hid_out, hid_in, parts, xin, zout, zin, sout, sin, total = refs[43:54]
-    zs, zr, xs, xr, ys, yr, hs, hr, os_, or_, rs, rr, ss, sr = refs[54:68]
-    kzs, kzr, kxs, kxr, hes, her, ns, nr, fs, fr, gs, gr, ts, tr, wsem, isem = refs[68:]
+    kbuf, vbuf, qbuf, run_max, run_acc, att_out, att_in, proj = refs[25:33]
+    normed_ref, stream_ref, tab_in = refs[33:36]
+    gate, up, down, sgate, sup, sdown = refs[36:42]
+    rows, hid_own, hid_out, hid_in, parts, xin, zout, zin, sout, sin, total = refs[42:53]
+    zs, zr, xs, xr, ys, yr, hs, hr, os_, or_, rs, rr, ss, sr = refs[53:67]
+    kzs, kzr, kxs, kxr, hes, her, ns, nr, fs, fr, gs, gr, ts, tr, wsem, isem = refs[67:]
     s, t, z, x, depth = grid_place(sp)
     count, width = normed_ref.shape
     quarter = own_gate.shape[1]
@@ -248,16 +249,24 @@
     mirror = (s, (1 - y) * 2 + c)
     partner = (s, y * 2 + 1 - c)
     opposite = (s, (1 - y) * 2 + 1 - c)
-    line = [(lax.rem(z + k, depth) * 2 + x, t) for k in range(1, depth)]
-    far_line = [(lax.rem(z + k, depth) * 2 + 1 - x, t) for k in range(1, depth)]
+    levels = [z, z + 1 - 2 * (z % 2), lax.rem(z + 2, depth), depth - 1 - z]
+    inner = (z > 0) & (z < depth - 1)
+    line = [(level * 2 + x, t) for level in levels]
+    far_line = [(level * 2 + 1 - x, t) for level in levels]
     first, second = pl.ds(0, quarter), pl.ds(quarter, quarter)
-    started = []
+    started, inner_started = [], []
 
     def send(source, target, send_sem, recv_sem, peer):
         copy = remote(source, target, send_sem, recv_sem, peer)
         copy.start()
         started.append(copy)
         return copy
+
+    def inner_send(describe, *key):
+        remote(*describe(*key)).start()
+        inner_started.append((describe, key))
+
+    relays = {1: (3, 2), 3: (1, 2), 2: (1, 3)}
 
     loads = [
         pltpu.make_async_copy(source, place, wsem.at[n])
@@ -273,7 +282,7 @@
             )
         )
     ]
-    peers = line + far_line + [across, mirror, partner, opposite]
+    peers = line[1:] + far_line[1:] + [across, mirror, partner, opposite]
     barrier = pltpu.get_barrier_semaphore()
     for peer in peers:
         pl.semaphore_signal(barrier, inc=1, device_id=peer, device_id_type=MESH)
@@ -301,7 +310,7 @@
     fetches[0].wait()
     fetches[1].wait()
     pl.semaphore_wait(barrier, len(peers))
-    keys_z, keys_x = {}, {}
+    keys_x = {}
 
     def send_keys_x(j):
         keys_x[j] = [
@@ -309,14 +318,30 @@
             for i, buf in enumerate((kbuf, vbuf))
         ]
 
-    slabs = [1, 3, 2] if depth == 4 else list(range(1, depth))
+    kv = (kbuf, vbuf)
+
+    def key_copy(i, source, target, peer):
+        return (
+            kv[i].at[source, 0],
+            kv[i].at[target, 0],
+            kzs.at[i, peer, target - 1],
+            kzr.at[i, target - 1],
+            line[peer],
+        )
+
+    def wait_keys(m):
+        for i in range(2):
+            remote(*key_copy(i, 0, m, 1)).wait_recv()
+
+    for i in range(2):
+        send(*key_copy(i, 0, 1, 1))
+
+    @pl.when(inner)
+    def _():
+        for i in range(2):
+            inner_send(key_copy, i, 0, 3, 3)
+
     send_keys_x(0)
-    for j in slabs:
-        k = depth - j
-        keys_z[j] = [
-            send(buf.at[0, 0], buf.at[j, 0], kzs.at[i, k - 1], kzr.at[i, k - 1], line[k - 1])
-            for i, buf in enumerate((kbuf, vbuf))
-        ]
     for n in (6, 0, 1, 2, 3, 4, 5):
         loads[n].start()
     pieces = fs.shape[0]
@@ -358,39 +383,51 @@
         for i in range(2):
             mine = (lane >= i * (lanes // 2)) & (lane < (i + 1) * (lanes // 2))
             qbuf[2 * a + i] = jnp.where(mine, head_query, jnp.zeros_like(head_query))
-    scale = (lanes // 2) ** (-0.5)
-
-    def attend(j, low=0, high=2):
-        if high == 2:
+    scale = (lanes // 2) ** (-0.5) * math.log2(math.e)
+    head_width = vbuf.shape[3]
+
+    def attend(j, side):
+        if side == 1:
             for copy in keys_x[j]:
                 copy.wait_recv()
-        keys = kbuf[j, low:high].reshape((high - low) * tokens, lanes)
-        values = vbuf[j, low:high].reshape((high - low) * tokens, vbuf.shape[3])
+        keys = kbuf[j, side]
+        ones = jnp.ones((tokens, lanes), jnp.bfloat16)
+        values = jnp.concatenate([vbuf[j, side], ones], axis=1)
         for m in range(2 * head_group):
             scores = scale * lax.dot_general(
                 qbuf[m], keys, (((1,), (1,)), ((), ())), preferred_element_type=jnp.float32
             )
             top = jnp.max(scores, axis=1, keepdims=True)
-            if j != 0:
+            if (j, side) != (0, 0):
                 old = run_max[m]
                 top = jnp.maximum(old, top)
-                shrink = jnp.exp(old - top)
-            weights = jnp.exp(scores - top)
-            row_sum = jnp.sum(weights, axis=1, keepdims=True)
-            update = jnp.dot(
-                weights.astype(jnp.bfloat16), values, preferred_element_type=jnp.float32
-            )
-            if j != 0:
-                row_sum = row_sum + run_sum[m] * shrink
+                shrink = jnp.exp2(old - top)
+            weights = jnp.exp2(scores - top).astype(jnp.bfloat16)
+            update = jnp.dot(weights, values, preferred_element_type=jnp.float32)
+            if (j, side) != (0, 0):
                 update = update + run_acc[m] * shrink
             run_max[m] = top
-            run_sum[m] = row_sum
             run_acc[m] = update
 
-    def relay_keys(j):
-        for copy in keys_z[j]:
-            copy.wait_recv()
-        send_keys_x(j)
+    def relay_inner(m):
+        @pl.when(inner)
+        def _():
+            if m != 1:
+                wait_keys(m)
+            for i in range(2):
+                inner_send(key_copy, i, m, relays[m][1], relays[m][0])
+
+    def relay_keys(m):
+        if m == 1:
+            wait_keys(m)
+            relay_inner(m)
+        else:
+
+            @pl.when(jnp.logical_not(inner))
+            def _():
+                wait_keys(m)
+
+        send_keys_x(m)
 
     def build_table():
         chosen = routes_ref[:, :count]
@@ -408,25 +445,32 @@
         tab_in[s] = table_ref[...]
         return [
             send(table_ref, tab_in.at[s], ts.at[n], tr.at[n], peer)
-            for n, peer in enumerate(line + far_line + [across])
+            for n, peer in enumerate(line[1:] + far_line[1:] + [across])
         ]
 
-    relay_keys(slabs[0])
+    attend(0, 0)
+    relay_keys(1)
+    relay_inner(3)
     send_far(2)
-    attend(0)
-    relay_keys(slabs[1])
-    attend(slabs[0])
+    attend(0, 1)
+    relay_inner(2)
+    attend(1, 0)
+    relay_keys(2)
+    attend(1, 1)
     send_far(3)
-    relay_keys(slabs[2])
-    attend(slabs[2], 0, 1)
+    attend(2, 0)
+    relay_keys(3)
     tables = build_table()
-    attend(slabs[1])
+    attend(3, 0)
     send_far(4)
-    attend(slabs[2], 1, 2)
+    attend(2, 1)
+    attend(3, 1)
+
+    def mapped(m):
+        return run_acc[m, :, :head_width] / run_acc[m, :, head_width:]
+
     for a in range(head_group):
-        value = run_acc[2 * a] / run_sum[2 * a] - lam_ref[a] * (
-            run_acc[2 * a + 1] / run_sum[2 * a + 1]
-        )
+        value = mapped(2 * a) - lam_ref[a] * mapped(2 * a + 1)
         rms = lax.rsqrt(jnp.mean(value * value, axis=1, keepdims=True) + norm_eps)
         att_out[a] = (value * rms * head_gain_ref[...]).astype(jnp.bfloat16)
     heads = [
@@ -457,7 +501,6 @@
     inverse = lax.rsqrt(jnp.mean(wide * wide, axis=1, keepdims=True) + norm_eps)
     normed_ref[...] = (wide * inverse * norm_gain_ref[...]).astype(jnp.bfloat16)
 
-    z_rows = {}
     x_rows, y_rows, diagonal, hids, x_outs, z_outs = {}, {}, {}, {}, {}, {}
     half_width = width // 2
     waited = set()
@@ -486,9 +529,42 @@
                 loads[n].wait()
                 near[n].wait_recv()
 
+    def level_copy(source, target, peer, h):
+        return (
+            own_rows(source, h),
+            part(rows.at[0, target, 0], h),
+            zs.at[peer, target - 1, h],
+            zr.at[target - 1, h],
+            line[peer],
+        )
+
+    def wait_level(m, h):
+        remote(*level_copy(0, m, 1, h)).wait_recv()
+
+    def level_arrived(m, h):
+        if ("level", m, h) not in waited:
+            waited.add(("level", m, h))
+            if m == 1:
+                wait_level(m, h)
+            else:
+
+                @pl.when(jnp.logical_not(inner))
+                def _():
+                    wait_level(m, h)
+
+    def ZF(m, h):
+        if m == 1:
+            level_arrived(m, h)
+
+        @pl.when(inner)
+        def _():
+            if m != 1:
+                wait_level(m, h)
+            inner_send(level_copy, m, relays[m][1], relays[m][0], h)
+
     def RX(j, h):
         if j != 0:
-            arrived(z_rows, (j, h))
+            level_arrived(j, h)
         x_rows[j, h] = send(
             own_rows(j, h), part(rows.at[0, j, 1], h), xs.at[j, h], xr.at[j, h], across
         )
@@ -498,11 +574,11 @@
         if j in by_z:
             arrived(y_rows, (0, h))
             y_rows[j, h] = send(
-                part(rows.at[1, 0, 0], h), part(rows.at[1, j, 0], h), *sems, line[depth - j - 1]
+                part(rows.at[1, 0, 0], h), part(rows.at[1, j, 0], h), *sems, line[j]
             )
             return
         if j != 0:
-            arrived(z_rows, (j, h))
+            level_arrived(j, h)
         y_rows[j, h] = send(own_rows(j, h), part(rows.at[1, j, 0], h), *sems, mirror)
 
     def RD(j, h):
@@ -517,7 +593,8 @@
 
     def HO(j, h):
         if j != 0:
-            arrived(z_rows, (j, 0), (j, 1))
+            level_arrived(j, 0)
+            level_arrived(j, 1)
         arrived(x_rows, (j, 0), (j, 1))
         loaded(0, 2)
         hid_own[j] = hidden_of(rows[0, j].reshape(2 * count, width), gate, up)
@@ -573,7 +650,7 @@
         ) + jnp.dot(
             hid_in[j], down[pl.ds(half, half), columns], preferred_element_type=jnp.float32
         )
-        base = lax.rem(z + j, depth) * 2
+        base = levels[j] * 2
         parts[j, 1, :, columns] = (value[count:] * route_column(base + 1 - x)).astype(
             jnp.bfloat16
         )
@@ -593,7 +670,7 @@
             part(zin.at[j - 1], h),
             rs.at[j - 1, h],
             rr.at[j - 1, h],
-            line[j - 1],
+            line[j],
         )
 
     shared_copy = []
@@ -611,19 +688,17 @@
     def SS(j, h):
         shared_copy.append(send(sout, sin, ss, sr, mirror))
 
-    actions = {f.__name__: f for f in (RX, RY, RD, HO, HP, FD, FO, SH, SS, DR, FR)}
+    actions = {f.__name__: f for f in (RX, RY, RD, HO, HP, FD, FO, SH, SS, DR, FR, ZF)}
     by_x, by_z, steps = moe_plan()
     rows[0, 0, 0] = normed_ref[...]
-    for j in slabs:
-        k = depth - j
+    for h in range(2):
+        send(*level_copy(0, 1, 1, h))
+
+    @pl.when(inner)
+    def _():
         for h in range(2):
-            z_rows[j, h] = send(
-                part(normed_ref, h),
-                part(rows.at[0, j, 0], h),
-                zs.at[k - 1, h],
-                zr.at[k - 1, h],
-                line[k - 1],
-            )
+            inner_send(level_copy, 0, 3, 3, h)
+
     for step in steps:
         number = int(step[2:3] or 0)
         actions[step[:2]](number, "ab".index(step[3:4] or "a"))
@@ -638,24 +713,31 @@
     for copy in started:
         copy.wait_send()
 
+    @pl.when(inner)
+    def _():
+        for describe, key in inner_started:
+            remote(*describe(*key)).wait_send()
+
 
 def moe_plan():
-    return (1, 2), (3,), [
+    return (0, 2, 3), (1,), [
         step
         for group in (
-            "RX0a RX0b FR6 FR7",
-            "RY1a RX1a RX1b RY1b",
-            "RY0b RY0a RX3a RX3b",
-            "RD1b RY2a DR RD1a",
-            "RY2b RD3a RY3b RX2a",
-            "SH RX2b HO0 RD2a",
-            "RY3a RD3b RD2b HP1",
-            "HO1 RD0a HP3 FD1a",
-            "FD1b RD0b HO3 HP2",
-            "FD3a SS FO1a HO2",
-            "FD3b FO1b FD2b FO3a",
-            "HP0 FD2a FO3b FO2b",
-            "FD0b FD0a FO2a",
+            "RX0b RY0b FR6 RY0a",
+            "RX0a FR7 RD0b ZF1a",
+            "ZF3a RX1a ZF1b ZF3b",
+            "RX1b ZF2a RY2a RX2a",
+            "ZF2b RX2b RY2b RY1a",
+            "RY3a RD2a RD2b RY3b",
+            "RD1b HO2 RD3a HO0",
+            "RD3b DR RX3a RY1b",
+            "HP2 HO1 RD1a RX3b",
+            "HP3 FD2b FD2a HP1",
+            "HO3 RD0a FO2b FD3b",
+            "FD1b FO2a SH FD3a",
+            "FO3b FD1a HP0 SS",
+            "FO1b FO3a FD0a FO1a",
+            "FD0b",
         )
         for step in group.split()
     ]
@@ -683,8 +765,7 @@
         ((depth, 2, tokens, value.shape[1]), bf16),
         ((maps, tokens, lanes), bf16),
         ((maps, tokens, 1), f32),
-        ((maps, tokens, 1), f32),
-        ((maps, tokens, value.shape[1]), f32),
+        ((maps, tokens, value.shape[1] + lanes), f32),
         ((head_group, tokens, value.shape[1]), bf16),
         ((tp * head_group, count, value.shape[1]), bf16),
         (large[0].shape, bf16),
@@ -725,14 +806,14 @@
             pltpu.VMEM(table, f32),
         ]
         + [pltpu.VMEM(shape, dtype) for shape, dtype in scratch]
-        + dma(depth - 1, 2)
+        + [pltpu.SemaphoreType.DMA((depth, depth - 1, 2)), pltpu.SemaphoreType.DMA((depth - 1, 2))]
         + dma(depth, 2)
         + dma(2 * depth, 2)
         + dma(depth)
         + dma(depth, 2)
         + dma(depth - 1, 2)
         + [pltpu.SemaphoreType.DMA] * 2
-        + dma(2, depth - 1)
+        + [pltpu.SemaphoreType.DMA((2, depth, depth - 1)), pltpu.SemaphoreType.DMA((2, depth - 1))]
         + dma(2, depth)
         + dma(tp - 1)
         + dma(6)

time: 84.9 us -> 81.5 us (0.960)
  Pallas kernels: 83.1 us -> 79.7 us
    pallas_call x1, Pallas kernels: 83.1 us -> 79.7 us  [run_whole(): pl.pallas_call(partial(whole_kernel, sp, tp), out_shape=jax.ShapeDtypeStr...]
where the time goes in v4:
time: 81.5 us; the launch traced here: 81.4 us
  Pallas kernels  79.7 us (98%)
  local copies, waits for them, and re-layouts  1.62 us (2%)
    pallas_call x1, Pallas kernels, run_whole(): pl.pallas_call(partial(whole_kernel, sp, tp), out_shape=jax.ShapeDtypeStr...  79.7 us

profile of v4, /device:TPU:0, one launch (start us, length us, event | category | flops | bytes accessed | tf_op | source)
XLA Modules:
  0.0 81.4 jit_solution(15189251376206392118)
XLA Ops:
  0.0 79.7 %shard_map.154 = bf16[48,2048]{1,0:T(8,128)(2,1)} custom-call(bf16[192,128]{1,0:T(8,128)(2,1)} %refs_0_.1, bf16[192,128]{1,0:T(8,128)(2,1)} %refs_1_.1, bf16[192,256]{1,0:T(8,128)(2,1)} %refs_2_.1, f32[2]{0:T(128)} %refs_3_.1, s32[4,192]{1,0:T(4,128)} %bitcast.11, f32[4,48]{1,0:T(4,128)} %bitcast.12, bf16[48,2048]{1,0:T(8,128)(2,1)} %refs_6_.1, ...), custom_call_target="tpu_custom_call" | custom-call | flops 7247757312 | bytes 30000000 | tf_op jit(solution)/shard_map/pallas_call | solution.py:793
  79.7 1.6 %copy.18 = bf16[48,2048]{1,0:T(8,128)(2,1)} copy(bf16[48,2048]{1,0:T(8,128)(2,1)} %shard_map.154) | data formatting | bytes 393216

commit v5 on v4

--- a/solution.py
+++ b/solution.py
@@ -345,7 +345,7 @@
     for n in (6, 0, 1, 2, 3, 4, 5):
         loads[n].start()
     pieces = fs.shape[0]
-    early = pieces - 2
+    early = pieces - 1
     piece = quarter // pieces
     far_down = []
 
@@ -563,6 +563,16 @@
             inner_send(level_copy, m, relays[m][1], relays[m][0], h)
 
     def RX(j, h):
+        if j in by_zx:
+            arrived(x_rows, (0, h))
+            x_rows[j, h] = send(
+                part(rows.at[0, 0, 1], h),
+                part(rows.at[0, j, 1], h),
+                xs.at[j, h],
+                xr.at[j, h],
+                line[j],
+            )
+            return
         if j != 0:
             level_arrived(j, h)
         x_rows[j, h] = send(
@@ -584,7 +594,10 @@
     def RD(j, h):
         sems = ys.at[depth + j, h], yr.at[depth + j, h]
         target = part(rows.at[1, j, 1], h)
-        if j in by_x:
+        if j in by_zd:
+            arrived(diagonal, (0, h))
+            diagonal[j, h] = send(part(rows.at[1, 0, 1], h), target, *sems, line[j])
+        elif j in by_x:
             arrived(y_rows, (j, h))
             diagonal[j, h] = send(part(rows.at[1, j, 0], h), target, *sems, across)
         else:
@@ -689,7 +702,7 @@
         shared_copy.append(send(sout, sin, ss, sr, mirror))
 
     actions = {f.__name__: f for f in (RX, RY, RD, HO, HP, FD, FO, SH, SS, DR, FR, ZF)}
-    by_x, by_z, steps = moe_plan()
+    by_x, (by_z, by_zx, by_zd), steps = moe_plan()
     rows[0, 0, 0] = normed_ref[...]
     for h in range(2):
         send(*level_copy(0, 1, 1, h))
@@ -720,24 +733,23 @@
 
 
 def moe_plan():
-    return (0, 2, 3), (1,), [
+    return (2, 3), ((1,), (1,), (1,)), [
         step
         for group in (
-            "RX0b RY0b FR6 RY0a",
-            "RX0a FR7 RD0b ZF1a",
-            "ZF3a RX1a ZF1b ZF3b",
-            "RX1b ZF2a RY2a RX2a",
-            "ZF2b RX2b RY2b RY1a",
-            "RY3a RD2a RD2b RY3b",
-            "RD1b HO2 RD3a HO0",
-            "RD3b DR RX3a RY1b",
-            "HP2 HO1 RD1a RX3b",
-            "HP3 FD2b FD2a HP1",
-            "HO3 RD0a FO2b FD3b",
-            "FD1b FO2a SH FD3a",
-            "FO3b FD1a HP0 SS",
-            "FO1b FO3a FD0a FO1a",
-            "FD0b",
+            "RX0b FR7 RX0a RY0a",
+            "RY0b ZF1a ZF3a ZF2a",
+            "RY2a RX2a ZF1b ZF3b",
+            "ZF2b RY2b RX2b RX1a",
+            "RY1a RY3a RD0a RD2a",
+            "RD0b RY3b RD2b RY1b",
+            "RX3a HO2 SH DR",
+            "RD3a HP2 RX3b HP0",
+            "RD3b RD1a HO0 RD1b",
+            "SS FD2b FD2a HP3",
+            "RX1b FD0a FO2b HO3",
+            "HP1 FD3b FO2a FD3a",
+            "HO1 FD1b FO3b FD1a",
+            "FD0b FO3a FO1b FO1a",
         )
         for step in group.split()
     ]

time: 81.5 us -> 80.4 us (0.987)
  Pallas kernels: 79.7 us -> 78.7 us
    pallas_call x1, Pallas kernels: 79.7 us -> 78.7 us  [run_whole(): pl.pallas_call(partial(whole_kernel, sp, tp), out_shape=jax.ShapeDtypeStr...]
where the time goes in v5:
time: 80.4 us; the launch traced here: 80.3 us
  Pallas kernels  78.7 us (98%)
  local copies, waits for them, and re-layouts  1.62 us (2%)
    pallas_call x1, Pallas kernels, run_whole(): pl.pallas_call(partial(whole_kernel, sp, tp), out_shape=jax.ShapeDtypeStr...  78.7 us
    unnamed x1, local copies, waits for them, and re-layouts  1.62 us

profile of v5, /device:TPU:0, one launch (start us, length us, event | category | flops | bytes accessed | tf_op | source)
XLA Modules:
  0.0 80.3 jit_solution(13387583553953704251)
XLA Ops:
  0.0 78.7 %shard_map.154 = bf16[48,2048]{1,0:T(8,128)(2,1)} custom-call(bf16[192,128]{1,0:T(8,128)(2,1)} %refs_0_.1, bf16[192,128]{1,0:T(8,128)(2,1)} %refs_1_.1, bf16[192,256]{1,0:T(8,128)(2,1)} %refs_2_.1, f32[2]{0:T(128)} %refs_3_.1, s32[4,192]{1,0:T(4,128)} %bitcast.11, f32[4,48]{1,0:T(4,128)} %bitcast.12, bf16[48,2048]{1,0:T(8,128)(2,1)} %refs_6_.1, ...), custom_call_target="tpu_custom_call" | custom-call | flops 7247757312 | bytes 30000000 | tf_op jit(solution)/shard_map/pallas_call | solution.py:805
  78.7 1.6 %copy.18 = bf16[48,2048]{1,0:T(8,128)(2,1)} copy(bf16[48,2048]{1,0:T(8,128)(2,1)} %shard_map.154) | data formatting | bytes 393216
